TPU v7x, 32 devices: a whole 2x2x4 slice. The times are simulated.
32 devices in a mesh: sp: 16 (over z, y, x), tp: 2 (over core).
Axes of the slice: x: 2, y: 2, z: 4, core: 2. Of those that a mesh axis runs over, the one named last changes fastest.
Arguments:
- residual_in: bfloat16 [4096, 2048], P(('sp', 'tp')), may hold values from -6 to 6
- query_lean: bfloat16 [4096, 8, 96], P('sp', 'tp'), may hold values from -60 to 60
- query_broad: bfloat16 [4096, 8, 160], P('sp', 'tp'), may hold values from -60 to 60
- latent: bfloat16 [4096, 256], P('sp'), may hold values from -6 to 6
- rope_key: bfloat16 [4096, 32], P('sp'), may hold values from -8 to 8
- latent_gain: float32 [256], replicated, may hold values from 0.1 to 1.9
- key_up_lean: bfloat16 [256, 8, 64], P(None, 'tp'), may hold values from -0.375 to 0.375
- key_up_broad: bfloat16 [256, 8, 128], P(None, 'tp'), may hold values from -0.375 to 0.375
- value_up_lean: bfloat16 [256, 8, 64], P(None, 'tp'), may hold values from -0.375 to 0.375
- value_up_broad: bfloat16 [256, 8, 128], P(None, 'tp'), may hold values from -0.375 to 0.375
- out_lean: bfloat16 [8, 64, 2048], P('tp'), may hold values from -0.15625 to 0.15625
- out_broad: bfloat16 [8, 128, 2048], P('tp'), may hold values from -0.15625 to 0.15625
- attn_gain: float32 [2048], replicated, may hold values from 0.1 to 1.9
- mlp_gain: float32 [2048], replicated, may hold values from 0.1 to 1.9
- gate_weight: bfloat16 [2048, 2816], P('sp', 'tp'), may hold values from -0.125 to 0.125
- up_weight: bfloat16 [2048, 2816], P('sp', 'tp'), may hold values from -0.125 to 0.125
- down_weight: bfloat16 [2816, 2048], P('tp', 'sp'), may hold values from -0.109375 to 0.109375
Outputs:
- layer_out: bfloat16 [4096, 2048], P(('sp', 'tp'))
All inputs are finite; a program needn't handle non-finite values.
Results may differ from a plain program's by a relative error of at most 0.015.
Values may be sent and summed in bfloat16 or wider, within the bound.
A program may use at most 128 MiB of HBM per device.

v0:
```python
import functools
import math

import jax
import jax.numpy as jnp
from jax import lax
from jax.experimental import pallas as pl
from jax.experimental.pallas import tpu as pltpu
from jax.sharding import PartitionSpec as P

THETA = 10000.0
EPS = 1e-06
NEGATIVE = -1e30


def rotate(values, positions):
    width = values.shape[-1]
    half = width // 2
    freqs = THETA ** (-2.0 * jnp.arange(half, dtype=jnp.float32) / width)
    angle = positions.astype(jnp.float32)[:, None] * freqs[None, :]
    cosine = jnp.cos(angle)
    sine = jnp.sin(angle)
    if values.ndim == 3:
        cosine = cosine[:, None, :]
        sine = sine[:, None, :]
    first = values[..., :half]
    second = values[..., half:]
    return jnp.concatenate(
        [first * cosine - second * sine, first * sine + second * cosine], axis=-1
    )


def normalize(values, gain):
    return values * lax.rsqrt(jnp.mean(values * values, axis=-1, keepdims=True) + EPS) * gain


def block_keys(weights, latent_rows):
    projected = []
    for key_up, value_up in weights:
        keys = jnp.einsum(
            "kr,rhd->khd", latent_rows, key_up, preferred_element_type=jnp.float32
        ).astype(jnp.bfloat16)
        values = jnp.einsum(
            "kr,rhd->khd", latent_rows, value_up, preferred_element_type=jnp.float32
        ).astype(jnp.bfloat16)
        projected.append((keys, values))
    return projected


def attend(carry, queries, projected, rotated_rows, key_pos, query_pos):
    updated = []
    visible = key_pos[None, :] <= query_pos[:, None]
    for state, query, pair in zip(carry, queries, projected):
        query_nope, query_rot, scale = query
        keys, values = pair
        peak, total, accum = state
        scores = (
            jnp.einsum("qhd,khd->hqk", query_nope, keys, preferred_element_type=jnp.float32)
            + jnp.einsum("qhr,kr->hqk", query_rot, rotated_rows, preferred_element_type=jnp.float32)
        ) * scale
        scores = jnp.where(visible[None], scores, NEGATIVE)
        new_peak = jnp.maximum(peak, jnp.max(scores, axis=-1))
        weights = jnp.where(visible[None], jnp.exp(scores - new_peak[..., None]), 0.0)
        factor = jnp.exp(peak - new_peak)
        total = total * factor + jnp.sum(weights, axis=-1)
        accum = accum * factor[..., None] + jnp.einsum(
            "hqk,khv->hqv", weights.astype(jnp.bfloat16), values, preferred_element_type=jnp.float32
        )
        updated.append((new_peak, total, accum))
    return tuple(updated)


def fold_piece(carry, latent_piece, rotated_piece, piece_pos, weights, segments):
    count = latent_piece.shape[0]
    block = math.gcd(count, 1024)
    last_all = segments[0][1][-1]

    def one_block(index, state):
        lat_rows = lax.dynamic_slice_in_dim(latent_piece, index * block, block, 0)
        rot_rows = lax.dynamic_slice_in_dim(rotated_piece, index * block, block, 0)
        pos_rows = lax.dynamic_slice_in_dim(piece_pos, index * block, block, 0)
        first_key = jnp.min(pos_rows)

        def work(inner):
            projected = block_keys(weights, lat_rows)
            results = []
            for inner_seg, segment in zip(inner, segments):
                queries, seg_pos = segment
                results.append(
                    lax.cond(
                        first_key <= seg_pos[-1],
                        lambda held, queries=queries, seg_pos=seg_pos: attend(
                            held, queries, projected, rot_rows, pos_rows, seg_pos
                        ),
                        lambda held: held,
                        inner_seg,
                    )
                )
            return tuple(results)

        return lax.cond(first_key <= last_all, work, lambda inner: inner, state)

    return lax.fori_loop(0, count // block, one_block, carry)


def shards(
    residual_in,
    query_lean,
    query_broad,
    latent,
    rope_key,
    latent_gain,
    key_up_lean,
    key_up_broad,
    value_up_lean,
    value_up_broad,
    out_lean,
    out_broad,
    attn_gain,
    mlp_gain,
    gate_weight,
    up_weight,
    down_weight,
):
    tokens_here = query_lean.shape[0]
    n_tp = lax.axis_size("tp")
    share = tokens_here // n_tp
    sp_index = lax.axis_index("sp")
    first = sp_index * tokens_here
    query_pos = first + jnp.arange(tokens_here, dtype=jnp.int32)
    rope_width = rope_key.shape[1]
    weights = ((key_up_lean, value_up_lean), (key_up_broad, value_up_broad))
    segment_rows = (query_lean, query_broad, query_pos)
    segments = []
    initial = []
    lean_rows, broad_rows, seg_pos = segment_rows
    queries = []
    states = []
    for query, value_up in ((lean_rows, value_up_lean), (broad_rows, value_up_broad)):
        nope = query.shape[2] - rope_width
        query_rot = rotate(query[:, :, nope:].astype(jnp.float32), seg_pos).astype(jnp.bfloat16)
        queries.append((query[:, :, :nope], query_rot, query.shape[2] ** (-0.5)))
        heads = query.shape[1]
        rows = query.shape[0]
        states.append(
            (
                jnp.full((heads, rows), NEGATIVE, jnp.float32),
                jnp.zeros((heads, rows), jnp.float32),
                jnp.zeros((heads, rows, value_up.shape[2]), jnp.float32),
            )
        )
    segments.append((tuple(queries), seg_pos))
    initial.append(tuple(states))
    segments = tuple(segments)
    initial = tuple(initial)
    sent_latent = normalize(latent.astype(jnp.float32), latent_gain).astype(jnp.bfloat16)
    sent_rot = rotate(rope_key.astype(jnp.float32), query_pos).astype(jnp.bfloat16)
    pieces = (
        lax.all_gather(sent_latent, "sp", axis=0, tiled=True),
        lax.all_gather(sent_rot, "sp", axis=0, tiled=True),
    )
    piece_pos = jnp.arange(pieces[0].shape[0], dtype=jnp.int32)
    folded = fold_piece(initial, pieces[0], pieces[1], piece_pos, weights, segments)
    results = [
        [(accum / total[..., None]).astype(jnp.bfloat16) for peak, total, accum in seg_state]
        for seg_state in folded
    ]
    attended = results[0]
    term = jnp.zeros((share * lax.axis_size("tp"), out_lean.shape[2]), jnp.float32)
    for rows_all, weight in ((attended[0], out_lean), (attended[1], out_broad)):
        rows = rows_all
        term = term + jnp.einsum("hqv,hvd->qd", rows, weight, preferred_element_type=jnp.float32)
    head_sum = lax.psum_scatter(
        term.astype(jnp.bfloat16), "tp", scatter_dimension=0, tiled=True
    ).astype(jnp.float32)
    branch = normalize(head_sum, attn_gain)
    kept = (residual_in.astype(jnp.float32) + branch).astype(jnp.bfloat16)
    normed = normalize(kept.astype(jnp.float32), mlp_gain).astype(jnp.bfloat16)
    whole_normed = lax.all_gather(normed, "tp", axis=0, tiled=True)
    gate_whole, up_whole, down_whole = (
        lax.all_gather(gate_weight, "sp", axis=0, tiled=True),
        lax.all_gather(up_weight, "sp", axis=0, tiled=True),
        lax.all_gather(down_weight, "sp", axis=1, tiled=True),
    )
    gate = jnp.dot(whole_normed, gate_whole, preferred_element_type=jnp.float32)
    up = jnp.dot(whole_normed, up_whole, preferred_element_type=jnp.float32)
    hidden = (jax.nn.silu(gate) * up).astype(jnp.bfloat16)
    rows = hidden
    channel_sum = lax.psum_scatter(
        jnp.dot(rows, down_whole, preferred_element_type=jnp.float32).astype(jnp.bfloat16),
        "tp",
        scatter_dimension=0,
        tiled=True,
    ).astype(jnp.float32)
    return (kept.astype(jnp.float32) + 0.5 * channel_sum).astype(jnp.bfloat16)


LOG2E = math.log2(math.e)


def grid_of(mesh):
    n_sp, n_tp = mesh.shape["sp"], mesh.shape["tp"]
    devices = mesh.devices.reshape(n_sp, n_tp)
    try:
        places = [tuple(device.coords) for device in devices[:, 0]]
        partners = [tuple(device.coords) for device in devices[:, -1]]
    except Exception:
        return (n_sp // 4, 2, 2) if n_sp % 4 == 0 else None
    if places != partners:
        return None
    low = [min(place[k] for place in places) for k in range(3)]
    sizes = [max(place[k] for place in places) - low[k] + 1 for k in range(3)]
    wide_z, wide_y, wide_x = sizes[2], sizes[1], sizes[0]
    if wide_z * wide_y * wide_x != n_sp:
        return None
    for index, place in enumerate(places):
        x, y, z = (place[k] - low[k] for k in range(3))
        if (z * wide_y + y) * wide_x + x != index:
            return None
    return wide_z, wide_y, wide_x


def hop_table(grid):
    wide_z = grid[0]
    entries = [
        (dz, fy, fx)
        for dz in range(1 - wide_z, wide_z)
        for fy in range(2)
        for fx in range(2)
        if (dz, fy, fx) != (0, 0, 0)
    ]
    entries.sort(key=lambda e: (abs(e[0]) + e[1] + e[2], abs(e[0]), e))
    return entries


def layer_kernel(
    grid, shapes, res_in, qlt, qbt, lat, cosine, sine, ag, mg, kul, kub, vul, vub, wol_in, wob_in, gw, uw, dw, out,
    lat_all, gate_all, up_all, down_all, ql, qb, ktl, ktb, valt_l, valt_b, peak, total, acc_l, acc_b, att, term, inbox, kept,
    normed, hidden, inbox2, wol, wob, res, lat_recv, lat_send, lat_pair, recv, send, own_sem, pair_send, pair_recv,
):
    wide_z, wide_y, wide_x = grid
    n_sp = wide_z * wide_y * wide_x
    tokens, share, rope = shapes
    heads_l, heads_b = qlt.shape[0], qbt.shape[0]
    bf16, f32 = jnp.bfloat16, jnp.float32
    me = lax.axis_index("sp")
    core = lax.axis_index("tp")
    my_x = lax.rem(me, wide_x)
    my_y = lax.rem(me // wide_x, wide_y)
    my_z = me // (wide_x * wide_y)
    here = (my_z, my_y, my_x)
    strides = (wide_y * wide_x, wide_x, 1)
    Z, Y, X = 0, 1, 2
    flip_y = me + (1 - 2 * my_y) * strides[1]
    flip_x = me + (1 - 2 * my_x)
    ways = (
        (X, None, None, flip_x),
        (Y, None, None, flip_y),
        (Z, -1, my_z > 0, jnp.maximum(me - strides[0], 0)),
        (Z, 1, my_z < wide_z - 1, jnp.minimum(me + strides[0], n_sp - 1)),
    )

    barrier = pltpu.get_barrier_semaphore()
    for dim, sign, exists, where in ways:
        def greet(where=where):
            pl.semaphore_signal(barrier, inc=1, device_id={"sp": where})
        if exists is None:
            greet()
        else:
            pl.when(exists)(greet)
    pl.semaphore_signal(barrier, inc=1, device_id={"tp": 1 - core})
    ends = jnp.where(my_z > 0, 1, 0) + jnp.where(my_z < wide_z - 1, 1, 0)
    pl.semaphore_wait(barrier, 3 + ends)

    def wanted(order, origin, way):
        dim, sign, exists, _ = way
        place = order.index(dim)
        ok = origin[dim] == here[dim] if sign is None else sign * (here[dim] - origin[dim]) >= 0
        for later in order[place + 1:]:
            ok = jnp.logical_and(ok, origin[later] == here[later])
        return ok if exists is None else jnp.logical_and(ok, exists)

    def index_of(origin):
        return origin[0] * strides[0] + origin[1] * strides[1] + origin[2]

    gate_rows, units = gw.shape
    down_cols = dw.shape[1]
    cut = units // 4
    ORDER_A, ORDER_B, ORDER_C, ORDER_D = (Z, X, Y), (Z, Y, X), (X, Y, Z), (Y, X, Z)

    def gate_at(ref):
        return lambda i: ref.at[pl.ds(pl.multiple_of(i * gate_rows, gate_rows), gate_rows)]

    def down_at(k):
        return lambda i: down_all.at[
            pl.ds(k * cut, cut), pl.ds(pl.multiple_of(i * down_cols, down_cols), down_cols)
        ]

    parts = [
        (ORDER_A, gw, gate_at(gate_all)),
        (ORDER_B, uw, gate_at(up_all)),
    ] + [
        (order, dw.at[pl.ds(k * cut, cut)], down_at(k))
        for k, order in enumerate((ORDER_A, ORDER_B, ORDER_C, ORDER_D))
    ]

    def part_copy(p, w, i, mine):
        order, own, at = parts[p]
        return pltpu.make_async_remote_copy(
            src_ref=own if mine else at(i), dst_ref=at(i), send_sem=send.at[p, w, i],
            recv_sem=recv.at[p, i], device_id={"sp": ways[w][3]},
        )

    half = lat.shape[0] // 2
    first = pl.multiple_of(core * half, half)

    def lat_at(i):
        return lat_all.at[i, pl.ds(first, half)]

    def lat_copy(w, i, mine):
        return pltpu.make_async_remote_copy(
            src_ref=lat.at[pl.ds(first, half)] if mine else lat_at(i), dst_ref=lat_at(i),
            send_sem=lat_send.at[w, i], recv_sem=lat_recv.at[i], device_id={"sp": ways[w][3]},
        )

    def pair_lat(i):
        return pltpu.make_async_remote_copy(
            src_ref=lat_at(i), dst_ref=lat_at(i), send_sem=lat_pair.at[0, i],
            recv_sem=lat_pair.at[1, i], device_id={"tp": 1 - core},
        )

    def run(condition, action):
        if condition is None:
            action()
        else:
            pl.when(condition)(action)

    for w, way in enumerate(ways):
        run(way[2], lambda w=w: lat_copy(w, me, True).start())
    own = [pltpu.make_async_copy(lat, lat_all.at[me], own_sem.at[0])]
    for p, (_, src, at) in enumerate(parts):
        own.append(pltpu.make_async_copy(src, at(me), own_sem.at[1 + p]))
    fetch = [
        pltpu.make_async_copy(src, dst, own_sem.at[1 + len(parts) + k])
        for k, (src, dst) in enumerate(((wol_in, wol), (wob_in, wob), (res_in, res)))
    ]
    for copy in own + fetch:
        copy.start()

    def send_own(w):
        for p in range(len(parts)):
            run(ways[w][2], lambda p=p: part_copy(p, w, me, True).start())

    send_own(0)

    table = hop_table(grid)
    codes = [((dz + wide_z - 1) * 2 + fy) * 2 + fx for dz, fy, fx in table]
    per = 4
    words = [
        sum(code << (7 * k) for k, code in enumerate(codes[at:at + per]))
        for at in range(0, len(codes), per)
    ]

    def origin_of(n):
        word = jnp.int32(words[0])
        for k in range(1, len(words)):
            word = jnp.where(n // per == k, jnp.int32(words[k]), word)
        rem = lax.rem(n, per)
        for k in range(1, per):
            word = jnp.where(rem >= k, word // 128, word)
        code = lax.rem(word, 128)
        dz = code // 4 - (wide_z - 1)
        fy = lax.rem(code // 2, 2)
        fx = lax.rem(code, 2)
        oz = my_z + dz
        oy = my_y + fy * (1 - 2 * my_y)
        ox = my_x + fx * (1 - 2 * my_x)
        return (oz, oy, ox), jnp.logical_and(oz >= 0, oz < wide_z)

    def lat_event(n, _):
        origin, valid = origin_of(n)

        @pl.when(valid)
        def _():
            i = index_of(origin)
            lat_copy(0, i, False).wait_recv()
            for w, way in enumerate(ways):
                run(wanted(ORDER_C, origin, way), lambda w=w: lat_copy(w, i, False).start())
            pair_lat(i).start()

        return 0

    def part_event(n, group):
        origin, valid = origin_of(n)

        @pl.when(valid)
        def _():
            i = index_of(origin)
            for p in group:
                part_copy(p, 0, i, False).wait_recv()
                for w, way in enumerate(ways):
                    run(
                        wanted(parts[p][0], origin, way),
                        lambda p=p, w=w: part_copy(p, w, i, False).start(),
                    )

    def events(low, high, group):
        def body(n, _):
            part_event(n, group)
            return 0

        lax.fori_loop(low, high, body, 0)

    soon, late = (0, 1, 4, 5), (2, 3)

    count = len(table)
    early = sum(1 for dz, fy, fx in table if abs(dz) + fy + fx <= 2)
    lax.fori_loop(0, early, lat_event, 0)
    send_own(1)
    lax.fori_loop(early, count, lat_event, 0)
    send_own(2)
    send_own(3)
    half_rope = rope // 2
    for given, query in ((qlt, ql), (qbt, qb)):
        nope = given.shape[1] - rope
        for h in range(given.shape[0]):
            one = given[h, nope:nope + half_rope, :].astype(f32)
            two = given[h, nope + half_rope:, :].astype(f32)
            query[h, :nope, :] = given[h, :nope, :]
            query[h, nope:nope + half_rope, :] = (one * cosine[...] - two * sine[...]).astype(bf16)
            query[h, nope + half_rope:, :] = (one * sine[...] + two * cosine[...]).astype(bf16)
    for copy in own:
        copy.wait()

    def lat_arrived(i, _):
        pl.when(i != me)(lambda: pair_lat(i).wait_recv())
        return 0

    lax.fori_loop(0, n_sp, lat_arrived, 0)

    peak[...] = jnp.full(peak.shape, NEGATIVE, f32)
    total[...] = jnp.zeros(total.shape, f32)
    acc_l[...] = jnp.zeros(acc_l.shape, f32)
    acc_b[...] = jnp.zeros(acc_b.shape, f32)
    wide_l = kul.shape[0] // heads_l
    wide_b = kub.shape[0] // heads_b
    contract = (((1,), (1,)), ((), ()))
    contract_rows = (((0,), (0,)), ((), ()))

    def attend_block(j, masked):
        rows = lat_all[j, :tokens, :]
        rot = lat_all[j, tokens:, :]
        for ups, keys, heads, wide in ((kul, ktl, heads_l, wide_l), (kub, ktb, heads_b, wide_b)):
            made = lax.dot_general(ups[...], rows, contract, preferred_element_type=f32).astype(bf16)
            for h in range(heads):
                keys[h, :wide, :] = made[h * wide:(h + 1) * wide]
                keys[h, wide:, :] = rot
        for ups, held in ((vul, valt_l), (vub, valt_b)):
            held[...] = lax.dot_general(
                ups[...], rows, contract, preferred_element_type=f32
            ).astype(bf16)
        if masked:
            key_pos = lax.broadcasted_iota(jnp.int32, (tokens, tokens), 0)
            visible = key_pos <= lax.broadcasted_iota(jnp.int32, (tokens, tokens), 1)
        for g in range(heads_l + heads_b):
            if g < heads_l:
                h, query, keys, held, acc, wide = g, ql, ktl, valt_l, acc_l, wide_l
            else:
                h, query, keys, held, acc, wide = g - heads_l, qb, ktb, valt_b, acc_b, wide_b
            scores = lax.dot_general(
                keys[h], query[h], contract_rows, preferred_element_type=f32
            ) * (LOG2E * query.shape[1] ** (-0.5))
            if masked:
                scores = jnp.where(visible, scores, NEGATIVE)
            old = peak[g]
            new = jnp.maximum(old, jnp.max(scores, axis=0, keepdims=True))
            weights = jnp.exp2(scores - new)
            factor = jnp.exp2(old - new)
            peak[g] = new
            total[g] = total[g] * factor + jnp.sum(weights, axis=0, keepdims=True)
            acc[h] = acc[h] * factor + jnp.dot(
                held[h * wide:(h + 1) * wide, :], weights.astype(bf16), preferred_element_type=f32
            )

    def step(j, _):
        events((j * early) // n_sp, ((j + 1) * early) // n_sp, soon)
        pl.when(j < me)(lambda: attend_block(j, False))
        return 0

    lax.fori_loop(0, n_sp, step, 0)
    attend_block(me, True)

    split = heads_l * wide_l
    for heads, wide, acc, base, col in (
        (heads_l, wide_l, acc_l, 0, 0), (heads_b, wide_b, acc_b, heads_l, split),
    ):
        together = wide_b // wide
        for h in range(0, heads, together):
            done = jnp.concatenate(
                [acc[h + k] / total[base + h + k] for k in range(together)], axis=0
            )
            att[:, col + h * wide:col + (h + together) * wide] = done.T.astype(bf16)

    features = out.shape[1]
    block = math.gcd(features, 512)

    for copy in fetch:
        copy.wait()

    def project(n, _):
        cols = pl.ds(pl.multiple_of(n * block, block), block)
        term[:, cols] = (
            jnp.dot(att[:, :split], wol[:, cols], preferred_element_type=f32)
            + jnp.dot(att[:, split:], wob[:, cols], preferred_element_type=f32)
        ).astype(bf16)
        return 0

    lax.fori_loop(0, features // block, project, 0)
    mine = pl.ds(pl.multiple_of(core * share, share), share)
    theirs = pl.ds(pl.multiple_of((1 - core) * share, share), share)

    def to_pair(k, src, dst):
        return pltpu.make_async_remote_copy(
            src_ref=src, dst_ref=dst, send_sem=pair_send.at[k], recv_sem=pair_recv.at[k],
            device_id={"tp": 1 - core},
        )

    heads_out = to_pair(0, term.at[theirs], inbox)
    heads_out.start()
    heads_out.wait_recv()
    rows_at_once = math.gcd(share, 16)

    def norms(n, _):
        rows = pl.ds(pl.multiple_of(n * rows_at_once, rows_at_once), rows_at_once)
        full = pl.ds(pl.multiple_of(core * share + n * rows_at_once, rows_at_once), rows_at_once)
        summed = term[full, :].astype(f32) + inbox[rows, :].astype(f32)
        branch = normalize(summed, ag[...])
        mixed = (res[rows, :].astype(f32) + branch).astype(bf16)
        kept[rows, :] = mixed
        normed[full, :] = normalize(mixed.astype(f32), mg[...]).astype(bf16)
        return 0

    lax.fori_loop(0, share // rows_at_once, norms, 0)
    rows_out = to_pair(1, normed.at[mine], normed.at[mine])
    rows_out.start()
    behind = min(early, count - early)

    def both_groups(n, _):
        part_event(n, soon)
        part_event(n - behind, late)
        return 0

    events(0, early - behind, late)
    lax.fori_loop(early, count, both_groups, 0)
    to_pair(1, normed.at[theirs], normed.at[theirs]).wait_recv()

    def feed(cols):
        gate = jnp.dot(normed[...], gate_all[:, cols], preferred_element_type=f32)
        up = jnp.dot(normed[...], up_all[:, cols], preferred_element_type=f32)
        hidden[:, cols] = (gate / (1.0 + jnp.exp(-gate)) * up).astype(bf16)

    span = 256
    chunks = units // span
    left = count - behind

    def feed_loop(n, _):
        events(left + (n * behind) // chunks, left + ((n + 1) * behind) // chunks, late)
        feed(pl.ds(pl.multiple_of(n * span, span), span))
        return 0

    lax.fori_loop(0, chunks, feed_loop, 0)
    if units % span:
        feed(pl.ds(units // span * span, units % span))
    heads_out.wait_send()
    wide_n = math.gcd(features, 256)

    def down(n, _):
        cols = pl.ds(pl.multiple_of(n * wide_n, wide_n), wide_n)
        term[:, cols] = jnp.dot(
            hidden[...], down_all[:, cols], preferred_element_type=f32
        ).astype(bf16)
        return 0

    lax.fori_loop(0, features // wide_n, down, 0)
    sums_out = to_pair(2, term.at[theirs], inbox2)
    sums_out.start()

    def sent(i, _):
        origin = (i // strides[0], lax.rem(i // strides[1], wide_y), lax.rem(i, wide_x))
        for w, way in enumerate(ways):
            run(wanted(ORDER_C, origin, way), lambda w=w: lat_copy(w, i, False).wait_send())
            for p, (order, _, _) in enumerate(parts):
                run(wanted(order, origin, way), lambda p=p, w=w: part_copy(p, w, i, False).wait_send())
        pl.when(i != me)(lambda: pair_lat(i).wait_send())
        return 0

    lax.fori_loop(0, n_sp, sent, 0)
    rows_out.wait_send()
    sums_out.wait_recv()

    def finish(n, _):
        rows = pl.ds(pl.multiple_of(n * rows_at_once, rows_at_once), rows_at_once)
        full = pl.ds(pl.multiple_of(core * share + n * rows_at_once, rows_at_once), rows_at_once)
        summed = term[full, :].astype(f32) + inbox2[rows, :].astype(f32)
        out[rows, :] = (kept[rows, :].astype(f32) + 0.5 * summed).astype(bf16)
        return 0

    lax.fori_loop(0, share // rows_at_once, finish, 0)
    sums_out.wait_send()


def fused_shards(
    grid, residual_in, query_lean, query_broad, latent, rope_key, latent_gain, key_up_lean,
    key_up_broad, value_up_lean, value_up_broad, out_lean, out_broad, attn_gain, mlp_gain,
    gate_weight, up_weight, down_weight,
):
    bf16, f32 = jnp.bfloat16, jnp.float32
    tokens = query_lean.shape[0]
    share, features = residual_in.shape
    rank = latent.shape[1]
    rope = rope_key.shape[1]
    n_sp = lax.axis_size("sp")
    positions = lax.axis_index("sp") * tokens + jnp.arange(tokens, dtype=jnp.int32)

    ql, qb = (jnp.transpose(query, (1, 2, 0)) for query in (query_lean, query_broad))
    freqs = THETA ** (-2.0 * jnp.arange(rope // 2, dtype=f32) / rope)
    angle = freqs[:, None] * positions.astype(f32)[None, :]
    lat = normalize(latent.astype(f32), latent_gain).astype(bf16)
    rot_key = rotate(rope_key.astype(f32), positions).astype(bf16)
    lat = jnp.concatenate([lat, rot_key.T], axis=0)
    kul = key_up_lean.reshape(rank, -1).T
    kub = key_up_broad.reshape(rank, -1).T
    vul = value_up_lean.reshape(rank, -1).T
    vub = value_up_broad.reshape(rank, -1).T
    wol = out_lean.reshape(-1, features)
    wob = out_broad.reshape(-1, features)
    heads = ql.shape[0] + qb.shape[0]
    units = gate_weight.shape[1]
    wide_b = value_up_broad.shape[2]
    vmem = pl.BlockSpec(memory_space=pltpu.VMEM)
    args = (
        residual_in, ql, qb, lat, jnp.cos(angle), jnp.sin(angle), attn_gain[None], mlp_gain[None],
        kul, kub, vul, vub, wol, wob,
        gate_weight, up_weight, down_weight,
    )
    dma = pltpu.SemaphoreType.DMA
    return pl.pallas_call(
        functools.partial(layer_kernel, grid, (tokens, share, rope)),
        out_shape=jax.ShapeDtypeStruct((share, features), bf16),
        in_specs=[
            pl.BlockSpec(memory_space=pl.ANY) if k in (0, 12, 13) else vmem for k in range(len(args))
        ],
        out_specs=vmem,
        scratch_shapes=[
            pltpu.VMEM((n_sp, tokens + rope, rank), bf16),
            pltpu.VMEM((features, units), bf16),
            pltpu.VMEM((features, units), bf16),
            pltpu.VMEM((units, features), bf16),
            pltpu.VMEM(ql.shape, bf16),
            pltpu.VMEM(qb.shape, bf16),
            pltpu.VMEM(ql.shape, bf16),
            pltpu.VMEM(qb.shape, bf16),
            pltpu.VMEM((vul.shape[0], tokens), bf16),
            pltpu.VMEM((vub.shape[0], tokens), bf16),
            pltpu.VMEM((heads, 1, tokens), f32),
            pltpu.VMEM((heads, 1, tokens), f32),
            pltpu.VMEM((ql.shape[0], value_up_lean.shape[2], tokens), f32),
            pltpu.VMEM((qb.shape[0], wide_b, tokens), f32),
            pltpu.VMEM((tokens, vul.shape[0] + vub.shape[0]), bf16),
            pltpu.VMEM((tokens, features), bf16),
            pltpu.VMEM((share, features), bf16),
            pltpu.VMEM((share, features), bf16),
            pltpu.VMEM((tokens, features), bf16),
            pltpu.VMEM((tokens, units), bf16),
            pltpu.VMEM((share, features), bf16),
            pltpu.VMEM(wol.shape, bf16),
            pltpu.VMEM(wob.shape, bf16),
            pltpu.VMEM(residual_in.shape, bf16),
            dma((n_sp,)),
            dma((4, n_sp)),
            dma((2, n_sp)),
            dma((6, n_sp)),
            dma((6, 4, n_sp)),
            dma((10,)),
            dma((3,)),
            dma((3,)),
        ],
        compiler_params=pltpu.CompilerParams(
            collective_id=0, has_side_effects=True, vmem_limit_bytes=62 * 2**20
        ),
    )(*args)


def fits(grid, mesh, args):
    if grid is None or mesh.shape["tp"] != 2 or grid[1] != 2 or grid[2] != 2 or grid[0] > 8:
        return False
    n_sp = mesh.shape["sp"]
    tokens = args[1].shape[0] // n_sp
    share = tokens // 2
    units = args[14].shape[1] // 2
    heads_l, heads_b = args[6].shape[1] // 2, args[7].shape[1] // 2
    wide_l, wide_b = args[6].shape[2], args[7].shape[2]
    rope = args[4].shape[1]
    return (
        tokens % 128 == 0 and tokens <= 256 and share % 16 == 0 and units >= 256
        and units % 64 == 0 and heads_l % 2 == 0 and 2 * wide_l == wide_b and wide_b % 128 == 0
        and args[3].shape[1] == tokens and rope % 32 == 0 and (tokens + rope) % 32 == 0
        and heads_b > 0 and args[8].shape[2] == wide_l and args[9].shape[2] == wide_b
        and (args[14].shape[0] // n_sp) % 16 == 0 and (args[16].shape[1] // n_sp) % 128 == 0
    )


def solution(mesh):
    in_specs = (
        P(("sp", "tp"), None),
        P("sp", "tp", None),
        P("sp", "tp", None),
        P("sp", None),
        P("sp", None),
        P(),
        P(None, "tp", None),
        P(None, "tp", None),
        P(None, "tp", None),
        P(None, "tp", None),
        P("tp", None, None),
        P("tp", None, None),
        P(),
        P(),
        P("sp", "tp"),
        P("sp", "tp"),
        P("tp", "sp"),
    )
    out_specs = P(("sp", "tp"), None)
    grid = grid_of(mesh)

    def layer(*args):
        body = functools.partial(fused_shards, grid) if fits(grid, mesh, args) else shards
        return jax.shard_map(
            body, mesh=mesh, in_specs=in_specs, out_specs=out_specs, check_vma=False
        )(*args)

    return layer
```

profile of v0, /device:TPU:27, one launch (start us, length us, event | category | flops | bytes accessed | tf_op | source)
XLA Modules:
  0.0 169.4 jit_solution(6159135581782157020)
XLA Ops:
  0.0 1.0 fusion
  1.1 0.7 convert_element_type.24
  1.8 0.1 fusion.8
  1.9 0.8 multiply_sine_fusion
  2.7 1.0 fusion.2
  3.7 0.7 pad_maximum_fusion.lat
  4.4 1.8 %copy.18 = bf16[256,4,128]{0,2,1:T(8,128)(2,1)} copy(bf16[256,4,128]{2,1,0:T(4,128)(2,1)} %param.24) | data formatting | bytes 524288 | tf_op args[7]
  6.2 1.8 %copy.19 = bf16[256,4,128]{0,2,1:T(8,128)(2,1)} copy(bf16[256,4,128]{2,1,0:T(4,128)(2,1)} %param.26) | data formatting | bytes 524288 | tf_op args[9]
  8.0 159.5 %shard_map.163 = bf16[128,2048]{1,0:T(8,128)(2,1)} custom-call(bf16[128,2048]{1,0:T(8,128)(2,1)} %res_in.1, bf16[4,96,256]{2,1,0:T(8,128)(2,1)} %bitcast.25, bf16[4,160,256]{2,1,0:T(8,128)(2,1)} %bitcast.24, bf16[288,256]{1,0:T(8,128)(2,1)} %pad_maximum_fusion.lat, f32[16,256]{1,0:T(8,128)} %get-tuple-element.8.cosine, f32[16,256]{1,0:T(8,128)} %get-tuple-element.7.sine, ...), custom_call_target="tpu_custom_call" | custom-call | tf_op jit(solution)/shard_map/pallas_call | solution.py:647
  167.5 1.9 %copy.21 = bf16[128,2048]{1,0:T(8,128)(2,1)} copy(bf16[128,2048]{1,0:T(8,128)(2,1)} %shard_map.163) | data formatting | bytes 1048576
  (4 shorter events, 0.0 us)
where the time goes:
time: 170 us; the launch traced here: 169 us
  Pallas kernels  159 us (94%)
  local copies, waits for them, and re-layouts  5.5 us (3%)
  other arithmetic  4.35 us (3%)
    pallas_call x1, Pallas kernels, fused_shards(): pl.pallas_call(functools.partial(layer_kernel, grid, (tokens, share, rope...  159 us
    unnamed x3, local copies, waits for them, and re-layouts  5.5 us

commit v1 on v0

--- a/solution.py
+++ b/solution.py
@@ -220,11 +220,11 @@
     return wide_z, wide_y, wide_x
 
 
-def hop_table(grid):
+def hop_table(grid, past):
     wide_z = grid[0]
     entries = [
         (dz, fy, fx)
-        for dz in range(1 - wide_z, wide_z)
+        for dz in range(1 - wide_z, 1 if past else wide_z)
         for fy in range(2)
         for fx in range(2)
         if (dz, fy, fx) != (0, 0, 0)
@@ -235,8 +235,9 @@
 
 def layer_kernel(
     grid, shapes, res_in, qlt, qbt, lat, cosine, sine, ag, mg, kul, kub, vul, vub, wol_in, wob_in, gw, uw, dw, out,
-    lat_all, gate_all, up_all, down_all, ql, qb, ktl, ktb, valt_l, valt_b, peak, total, acc_l, acc_b, att, term, inbox, kept,
-    normed, hidden, inbox2, wol, wob, res, lat_recv, lat_send, lat_pair, recv, send, own_sem, pair_send, pair_recv,
+    lat_all, gate_all, up_all, down_all, ext_all, own_g, own_u, own_d, own_e, ql, qb, ktl, ktb, valt_l, valt_b,
+    peak, total, acc_l, acc_b, att, term, inbox, kept, rows_all, hidden, inbox2, psum, inbox3, wol, wob, res,
+    lat_recv, lat_send, lat_pair, recv, send, own_sem, pair_send, pair_recv,
 ):
     wide_z, wide_y, wide_x = grid
     n_sp = wide_z * wide_y * wide_x
@@ -248,120 +249,94 @@
     my_x = lax.rem(me, wide_x)
     my_y = lax.rem(me // wide_x, wide_y)
     my_z = me // (wide_x * wide_y)
-    here = (my_z, my_y, my_x)
-    strides = (wide_y * wide_x, wide_x, 1)
-    Z, Y, X = 0, 1, 2
-    flip_y = me + (1 - 2 * my_y) * strides[1]
+    layer = wide_y * wide_x
+    flip_y = me + (1 - 2 * my_y) * wide_x
     flip_x = me + (1 - 2 * my_x)
-    ways = (
-        (X, None, None, flip_x),
-        (Y, None, None, flip_y),
-        (Z, -1, my_z > 0, jnp.maximum(me - strides[0], 0)),
-        (Z, 1, my_z < wide_z - 1, jnp.minimum(me + strides[0], n_sp - 1)),
-    )
-
-    barrier = pltpu.get_barrier_semaphore()
-    for dim, sign, exists, where in ways:
-        def greet(where=where):
-            pl.semaphore_signal(barrier, inc=1, device_id={"sp": where})
-        if exists is None:
-            greet()
-        else:
-            pl.when(exists)(greet)
-    pl.semaphore_signal(barrier, inc=1, device_id={"tp": 1 - core})
-    ends = jnp.where(my_z > 0, 1, 0) + jnp.where(my_z < wide_z - 1, 1, 0)
-    pl.semaphore_wait(barrier, 3 + ends)
-
-    def wanted(order, origin, way):
-        dim, sign, exists, _ = way
-        place = order.index(dim)
-        ok = origin[dim] == here[dim] if sign is None else sign * (here[dim] - origin[dim]) >= 0
-        for later in order[place + 1:]:
-            ok = jnp.logical_and(ok, origin[later] == here[later])
-        return ok if exists is None else jnp.logical_and(ok, exists)
-
-    def index_of(origin):
-        return origin[0] * strides[0] + origin[1] * strides[1] + origin[2]
+    side = lax.rem(my_z, 2)
+    partner = me + (1 - 2 * side) * layer
+    z_ways = [
+        (step, my_z + step < wide_z if step > 0 else my_z + step >= 0,
+         jnp.clip(me + step * layer, 0, n_sp - 1))
+        for step in (1, -1, 2, -2)
+    ]
+
+    def z_way(step):
+        return next(way for way in z_ways if way[0] == step)
+
+    def run(condition, action):
+        pl.when(condition)(action)
 
     gate_rows, units = gw.shape
     down_cols = dw.shape[1]
-    cut = units // 4
-    ORDER_A, ORDER_B, ORDER_C, ORDER_D = (Z, X, Y), (Z, Y, X), (X, Y, Z), (Y, X, Z)
-
-    def gate_at(ref):
-        return lambda i: ref.at[pl.ds(pl.multiple_of(i * gate_rows, gate_rows), gate_rows)]
-
-    def down_at(k):
-        return lambda i: down_all.at[
-            pl.ds(k * cut, cut), pl.ds(pl.multiple_of(i * down_cols, down_cols), down_cols)
-        ]
-
-    parts = [
-        (ORDER_A, gw, gate_at(gate_all)),
-        (ORDER_B, uw, gate_at(up_all)),
-    ] + [
-        (order, dw.at[pl.ds(k * cut, cut)], down_at(k))
-        for k, order in enumerate((ORDER_A, ORDER_B, ORDER_C, ORDER_D))
+    main = gate_all.shape[1]
+    extra = units - 2 * main
+    fetch = [
+        pltpu.make_async_copy(src, dst, own_sem.at[k])
+        for k, (src, dst) in enumerate((
+            (gw, own_g), (uw, own_u), (dw, own_d),
+            (gw.at[:, pl.ds(2 * main, extra)], own_e.at[0]),
+            (uw.at[:, pl.ds(2 * main, extra)], own_e.at[1]),
+            (dw.at[pl.ds(2 * main, extra), :], own_e.at[2]),
+            (wol_in, wol), (wob_in, wob), (res_in, res),
+        ))
     ]
-
-    def part_copy(p, w, i, mine):
-        order, own, at = parts[p]
-        return pltpu.make_async_remote_copy(
-            src_ref=own if mine else at(i), dst_ref=at(i), send_sem=send.at[p, w, i],
-            recv_sem=recv.at[p, i], device_id={"sp": ways[w][3]},
-        )
-
-    half = lat.shape[0] // 2
-    first = pl.multiple_of(core * half, half)
+    lat_rows = lat.shape[0]
+    own_lat = pltpu.make_async_copy(
+        lat, lat_all.at[pl.ds(pl.multiple_of(me * lat_rows, lat_rows), lat_rows)], own_sem.at[len(fetch)]
+    )
+    for copy in fetch:
+        copy.start()
+    own_lat.start()
+
+    barrier = pltpu.get_barrier_semaphore()
+    for where in (flip_x, flip_y):
+        pl.semaphore_signal(barrier, inc=1, device_id={"sp": where})
+    pl.semaphore_signal(barrier, inc=1, device_id={"tp": 1 - core})
+    greeted = 3
+    for _, exists, where in z_ways:
+        run(exists, lambda where=where: pl.semaphore_signal(barrier, inc=1, device_id={"sp": where}))
+        greeted = greeted + jnp.where(exists, 1, 0)
+    pl.semaphore_wait(barrier, greeted)
+
+    half = lat_rows // 2
+    first = pl.multiple_of(core * half, 16)
 
     def lat_at(i):
-        return lat_all.at[i, pl.ds(first, half)]
-
-    def lat_copy(w, i, mine):
+        return lat_all.at[pl.ds(pl.multiple_of(i * lat_rows + first, 16), half)]
+
+    def lat_copy(i, mine, where):
         return pltpu.make_async_remote_copy(
             src_ref=lat.at[pl.ds(first, half)] if mine else lat_at(i), dst_ref=lat_at(i),
-            send_sem=lat_send.at[w, i], recv_sem=lat_recv.at[i], device_id={"sp": ways[w][3]},
+            send_sem=lat_send.at[0], recv_sem=lat_recv.at[i], device_id={"sp": where},
         )
 
     def pair_lat(i):
         return pltpu.make_async_remote_copy(
-            src_ref=lat_at(i), dst_ref=lat_at(i), send_sem=lat_pair.at[0, i],
-            recv_sem=lat_pair.at[1, i], device_id={"tp": 1 - core},
+            src_ref=lat_at(i), dst_ref=lat_at(i), send_sem=lat_send.at[1],
+            recv_sem=lat_pair.at[i], device_id={"tp": 1 - core},
         )
 
-    def run(condition, action):
-        if condition is None:
-            action()
-        else:
-            pl.when(condition)(action)
-
-    for w, way in enumerate(ways):
-        run(way[2], lambda w=w: lat_copy(w, me, True).start())
-    own = [pltpu.make_async_copy(lat, lat_all.at[me], own_sem.at[0])]
-    for p, (_, src, at) in enumerate(parts):
-        own.append(pltpu.make_async_copy(src, at(me), own_sem.at[1 + p]))
-    fetch = [
-        pltpu.make_async_copy(src, dst, own_sem.at[1 + len(parts) + k])
-        for k, (src, dst) in enumerate(((wol_in, wol), (wob_in, wob), (res_in, res)))
-    ]
-    for copy in own + fetch:
-        copy.start()
-
-    def send_own(w):
-        for p in range(len(parts)):
-            run(ways[w][2], lambda p=p: part_copy(p, w, me, True).start())
-
-    send_own(0)
-
-    table = hop_table(grid)
-    codes = [((dz + wide_z - 1) * 2 + fy) * 2 + fx for dz, fy, fx in table]
+    def lat_forward(i, fy, fx, mine):
+        column = jnp.logical_and(fy == 0, fx == 0)
+        up = z_way(1)
+        run(jnp.logical_and(column, up[1]), lambda: lat_copy(i, mine, up[2]).start())
+        to_x = jnp.logical_or(column, jnp.logical_and(core == 1, jnp.logical_and(fy == 1, fx == 0)))
+        to_y = jnp.logical_or(column, jnp.logical_and(core == 0, jnp.logical_and(fy == 0, fx == 1)))
+        run(to_x, lambda: lat_copy(i, mine, flip_x).start())
+        run(to_y, lambda: lat_copy(i, mine, flip_y).start())
+
+    lat_forward(me, my_y * 0, my_x * 0, True)
+
     per = 4
-    words = [
-        sum(code << (7 * k) for k, code in enumerate(codes[at:at + per]))
-        for at in range(0, len(codes), per)
-    ]
-
-    def origin_of(n):
+
+    def words_of(table):
+        codes = [((dz + wide_z - 1) * 2 + fy) * 2 + fx for dz, fy, fx in table]
+        return [
+            sum(code << (7 * k) for k, code in enumerate(codes[at:at + per]))
+            for at in range(0, len(codes), per)
+        ]
+
+    def origin_of(n, words):
         word = jnp.int32(words[0])
         for k in range(1, len(words)):
             word = jnp.where(n // per == k, jnp.int32(words[k]), word)
@@ -369,57 +344,155 @@
         for k in range(1, per):
             word = jnp.where(rem >= k, word // 128, word)
         code = lax.rem(word, 128)
-        dz = code // 4 - (wide_z - 1)
-        fy = lax.rem(code // 2, 2)
-        fx = lax.rem(code, 2)
-        oz = my_z + dz
+        return code // 4 - (wide_z - 1), lax.rem(code // 2, 2), lax.rem(code, 2)
+
+    def index_of(dz, fy, fx):
         oy = my_y + fy * (1 - 2 * my_y)
         ox = my_x + fx * (1 - 2 * my_x)
-        return (oz, oy, ox), jnp.logical_and(oz >= 0, oz < wide_z)
+        return ((my_z + dz) * wide_y + oy) * wide_x + ox
+
+    past = hop_table(grid, True)
+    past_words = words_of(past)
 
     def lat_event(n, _):
-        origin, valid = origin_of(n)
-
-        @pl.when(valid)
+        dz, fy, fx = origin_of(n, past_words)
+
+        @pl.when(my_z + dz >= 0)
         def _():
-            i = index_of(origin)
-            lat_copy(0, i, False).wait_recv()
-            for w, way in enumerate(ways):
-                run(wanted(ORDER_C, origin, way), lambda w=w: lat_copy(w, i, False).start())
+            i = index_of(dz, fy, fx)
+            lat_copy(i, False, flip_x).wait_recv()
+            lat_forward(i, fy, fx, False)
             pair_lat(i).start()
 
         return 0
 
-    def part_event(n, group):
-        origin, valid = origin_of(n)
-
-        @pl.when(valid)
+    lax.fori_loop(0, len(past), lat_event, 0)
+
+    def slot_at(ref, i):
+        return ref.at[pl.ds(pl.multiple_of(i * gate_rows, gate_rows), gate_rows)]
+
+    def down_slot(dz, fy, fx):
+        slot = (fy * 2 + fx) * wide_z + my_z + dz
+        return down_all.at[pl.ds(0, main), pl.ds(pl.multiple_of(slot * down_cols, down_cols), down_cols)]
+
+    def place(p, dz, fy, fx):
+        i = index_of(dz, fy, fx)
+        if p == 0:
+            return slot_at(gate_all, i)
+        if p == 1:
+            return slot_at(up_all, i)
+        if p == 2:
+            return down_slot(dz, fy, fx)
+        return ext_all.at[i]
+
+    def own_half(p, h):
+        lanes = pl.ds(pl.multiple_of(h * main, extra), main)
+        if p == 0:
+            return own_g.at[:, lanes]
+        if p == 1:
+            return own_u.at[:, lanes]
+        if p == 2:
+            return own_d.at[lanes, :]
+        return own_e
+
+    def part_copy(p, src, dst, i, where):
+        return pltpu.make_async_remote_copy(
+            src_ref=src, dst_ref=dst, send_sem=send.at[p], recv_sem=recv.at[p, i], device_id={"sp": where},
+        )
+
+    has_extra = core == side
+    x_first = (True, False, core == 0, False)
+
+    def to_z(p, src, step, origin, i, condition=True):
+        _, exists, where = z_way(step)
+        dst = place(p, *origin) if p == 2 else place(p, *origin)
+        run(jnp.logical_and(exists, condition), lambda: part_copy(p, src, dst, i, where).start())
+
+    def seen(origin, fy, fx):
+        return origin[0], origin[1] + fy - 2 * origin[1] * fy, origin[2] + fx - 2 * origin[2] * fx
+
+    def dst_for(p, origin, fy, fx):
+        if p == 2:
+            return down_slot(*seen(origin, fy, fx))
+        return place(p, *origin)
+
+    def send_own(p):
+        here = (0, 0, 0)
+        mine = own_half(p, side)
+        other = own_half(p, 1 - side)
+        same = has_extra if p == 3 else True
+        cross = jnp.logical_not(has_extra) if p == 3 else True
+        for step in (1, -1):
+            to_z(p, other, step, here, me, cross)
+        for step in (2, -2):
+            to_z(p, mine, step, here, me, same)
+
+        def flips():
+            part_copy(p, mine, dst_for(p, here, 0, 1), me, flip_x).start()
+            part_copy(p, mine, dst_for(p, here, 1, 0), me, flip_y).start()
+
+        if p == 3:
+            run(has_extra, flips)
+        else:
+            flips()
+
+    def part_event(p, dz, fy, fx):
+        origin = (dz, fy, fx)
+        i = index_of(*origin)
+        here = place(p, *origin)
+        part_copy(p, here, here, i, flip_x).wait_recv()
+        column = jnp.logical_and(fy == 0, fx == 0)
+        to_z(p, here, 2, origin, i, jnp.logical_and(column, dz < 0))
+        to_z(p, here, -2, origin, i, jnp.logical_and(column, dz > 0))
+        x_line = jnp.logical_and(fy == 0, fx == 1)
+        y_line = jnp.logical_and(fy == 1, fx == 0)
+        if x_first[p] is True:
+            to_x, to_y = column, jnp.logical_or(column, x_line)
+        elif x_first[p] is False:
+            to_x, to_y = jnp.logical_or(column, y_line), column
+        else:
+            to_x = jnp.logical_or(column, jnp.logical_and(y_line, jnp.logical_not(x_first[p])))
+            to_y = jnp.logical_or(column, jnp.logical_and(x_line, x_first[p]))
+        run(to_x, lambda: part_copy(p, here, dst_for(p, origin, 0, 1), i, flip_x).start())
+        run(to_y, lambda: part_copy(p, here, dst_for(p, origin, 1, 0), i, flip_y).start())
+
+    for copy in fetch[:6]:
+        copy.wait()
+    for p in (0, 1, 3):
+        send_own(p)
+
+    whole = hop_table(grid, False)
+    whole_words = words_of(whole)
+
+    def gate_event(n, _):
+        dz, fy, fx = origin_of(n, whole_words)
+
+        @pl.when(jnp.logical_and(my_z + dz >= 0, my_z + dz < wide_z))
         def _():
-            i = index_of(origin)
-            for p in group:
-                part_copy(p, 0, i, False).wait_recv()
-                for w, way in enumerate(ways):
-                    run(
-                        wanted(parts[p][0], origin, way),
-                        lambda p=p, w=w: part_copy(p, w, i, False).start(),
-                    )
-
-    def events(low, high, group):
-        def body(n, _):
-            part_event(n, group)
+            part_event(0, dz, fy, fx)
+            part_event(1, dz, fy, fx)
+            run(has_extra, lambda: part_event(3, dz, fy, fx))
+
+        return 0
+
+    def down_group(fy, fx):
+        def body(t, _):
+            dz = jnp.where(lax.rem(t, 2) == 1, -((t + 1) // 2), t // 2)
+            ok = jnp.logical_and(my_z + dz >= 0, my_z + dz < wide_z)
+            if (fy, fx) == (0, 0):
+                ok = jnp.logical_and(ok, dz != 0)
+            run(ok, lambda: part_event(2, dz, jnp.int32(fy), jnp.int32(fx)))
             return 0
 
-        lax.fori_loop(low, high, body, 0)
-
-    soon, late = (0, 1, 4, 5), (2, 3)
-
-    count = len(table)
-    early = sum(1 for dz, fy, fx in table if abs(dz) + fy + fx <= 2)
-    lax.fori_loop(0, early, lat_event, 0)
-    send_own(1)
-    lax.fori_loop(early, count, lat_event, 0)
-    send_own(2)
-    send_own(3)
+        lax.fori_loop(0, 2 * wide_z - 1, body, 0)
+
+    own_rows = pl.ds(pl.multiple_of(me * gate_rows, gate_rows), gate_rows)
+    own_lanes = pl.ds(pl.multiple_of(side * main, extra), main)
+    gate_all[own_rows, :] = own_g[:, own_lanes]
+    up_all[own_rows, :] = own_u[:, own_lanes]
+    down_all[:main, pl.ds(pl.multiple_of(my_z * down_cols, down_cols), down_cols)] = own_d[own_lanes, :]
+    ext_all[me] = own_e[...]
+
     half_rope = rope // 2
     for given, query in ((qlt, ql), (qbt, qb)):
         nope = given.shape[1] - rope
@@ -429,11 +502,11 @@
             query[h, :nope, :] = given[h, :nope, :]
             query[h, nope:nope + half_rope, :] = (one * cosine[...] - two * sine[...]).astype(bf16)
             query[h, nope + half_rope:, :] = (one * sine[...] + two * cosine[...]).astype(bf16)
-    for copy in own:
-        copy.wait()
+    own_lat.wait()
 
     def lat_arrived(i, _):
-        pl.when(i != me)(lambda: pair_lat(i).wait_recv())
+        ours = jnp.logical_and(i != me, i < (my_z + 1) * layer)
+        run(ours, lambda: pair_lat(i).wait_recv())
         return 0
 
     lax.fori_loop(0, n_sp, lat_arrived, 0)
@@ -448,8 +521,9 @@
     contract_rows = (((0,), (0,)), ((), ()))
 
     def attend_block(j, masked):
-        rows = lat_all[j, :tokens, :]
-        rot = lat_all[j, tokens:, :]
+        at_j = pl.multiple_of(j * lat_rows, 16)
+        rows = lat_all[pl.ds(at_j, tokens), :]
+        rot = lat_all[pl.ds(pl.multiple_of(at_j + tokens, 16), rope), :]
         for ups, keys, heads, wide in ((kul, ktl, heads_l, wide_l), (kub, ktb, heads_b, wide_b)):
             made = lax.dot_general(ups[...], rows, contract, preferred_element_type=f32).astype(bf16)
             for h in range(heads):
@@ -483,12 +557,16 @@
             )
 
     def step(j, _):
-        events((j * early) // n_sp, ((j + 1) * early) // n_sp, soon)
+        lax.fori_loop((j * early) // n_sp, ((j + 1) * early) // n_sp, gate_event, 0)
         pl.when(j < me)(lambda: attend_block(j, False))
         return 0
 
+    count = len(whole)
+    early = sum(1 for dz, fy, fx in whole if abs(dz) + fy + fx <= 2)
     lax.fori_loop(0, n_sp, step, 0)
     attend_block(me, True)
+    send_own(2)
+    lax.fori_loop(early, count, gate_event, 0)
 
     split = heads_l * wide_l
     for heads, wide, acc, base, col in (
@@ -504,19 +582,18 @@
     features = out.shape[1]
     block = math.gcd(features, 512)
 
-    for copy in fetch:
+    for copy in fetch[6:]:
         copy.wait()
 
     def project(n, _):
         cols = pl.ds(pl.multiple_of(n * block, block), block)
-        term[:, cols] = (
+        term[:tokens, cols] = (
             jnp.dot(att[:, :split], wol[:, cols], preferred_element_type=f32)
             + jnp.dot(att[:, split:], wob[:, cols], preferred_element_type=f32)
         ).astype(bf16)
         return 0
 
     lax.fori_loop(0, features // block, project, 0)
-    mine = pl.ds(pl.multiple_of(core * share, share), share)
     theirs = pl.ds(pl.multiple_of((1 - core) * share, share), share)
 
     def to_pair(k, src, dst):
@@ -525,6 +602,15 @@
             device_id={"tp": 1 - core},
         )
 
+    def to_partner(k, src, dst):
+        return pltpu.make_async_remote_copy(
+            src_ref=src, dst_ref=dst, send_sem=pair_send.at[k], recv_sem=pair_recv.at[k],
+            device_id={"sp": partner},
+        )
+
+    def place_of(of_core, of_side):
+        return pl.ds(pl.multiple_of((of_core * 2 + of_side) * share, share), share)
+
     heads_out = to_pair(0, term.at[theirs], inbox)
     heads_out.start()
     heads_out.wait_recv()
@@ -533,80 +619,156 @@
     def norms(n, _):
         rows = pl.ds(pl.multiple_of(n * rows_at_once, rows_at_once), rows_at_once)
         full = pl.ds(pl.multiple_of(core * share + n * rows_at_once, rows_at_once), rows_at_once)
+        spot = pl.ds(pl.multiple_of((core * 2 + side) * share + n * rows_at_once, rows_at_once), rows_at_once)
         summed = term[full, :].astype(f32) + inbox[rows, :].astype(f32)
         branch = normalize(summed, ag[...])
         mixed = (res[rows, :].astype(f32) + branch).astype(bf16)
         kept[rows, :] = mixed
-        normed[full, :] = normalize(mixed.astype(f32), mg[...]).astype(bf16)
+        rows_all[spot, :] = normalize(mixed.astype(f32), mg[...]).astype(bf16)
         return 0
 
     lax.fori_loop(0, share // rows_at_once, norms, 0)
-    rows_out = to_pair(1, normed.at[mine], normed.at[mine])
+    mine_at = rows_all.at[place_of(core, side)]
+    rows_out = to_pair(1, mine_at, mine_at)
+    rows_far = to_partner(2, mine_at, mine_at)
     rows_out.start()
-    behind = min(early, count - early)
-
-    def both_groups(n, _):
-        part_event(n, soon)
-        part_event(n - behind, late)
+    rows_far.start()
+    heads_out.wait_send()
+    far_at = rows_all.at[place_of(core, 1 - side)]
+    to_partner(2, far_at, far_at).wait_recv()
+    rows_on = to_pair(3, far_at, far_at)
+    rows_on.start()
+    near_at = rows_all.at[place_of(1 - core, side)]
+    to_pair(1, near_at, near_at).wait_recv()
+    last_at = rows_all.at[place_of(1 - core, 1 - side)]
+    to_pair(3, last_at, last_at).wait_recv()
+    down_group(0, 0)
+
+    def feed_from(rows, gate_w, up_w, cols):
+        gate = jnp.dot(rows_all[rows, :], gate_w, preferred_element_type=f32)
+        up = jnp.dot(rows_all[rows, :], up_w, preferred_element_type=f32)
+        hidden[rows, cols] = (gate / (1.0 + jnp.exp(-gate)) * up).astype(bf16)
+
+    span = math.gcd(main, 256)
+    chunks = main // span
+    group = 2 * tokens // 2
+
+    def group_rows(n):
+        return pl.ds(pl.multiple_of(n * group, group), group)
+
+    def feed_loop(n, _):
+        rows = group_rows(n // chunks)
+        cols = pl.ds(pl.multiple_of(lax.rem(n, chunks) * span, span), span)
+        feed_from(rows, gate_all[:, cols], up_all[:, cols], cols)
         return 0
 
-    events(0, early - behind, late)
-    lax.fori_loop(early, count, both_groups, 0)
-    to_pair(1, normed.at[theirs], normed.at[theirs]).wait_recv()
-
-    def feed(cols):
-        gate = jnp.dot(normed[...], gate_all[:, cols], preferred_element_type=f32)
-        up = jnp.dot(normed[...], up_all[:, cols], preferred_element_type=f32)
-        hidden[:, cols] = (gate / (1.0 + jnp.exp(-gate)) * up).astype(bf16)
-
-    span = 256
-    chunks = units // span
-    left = count - behind
-
-    def feed_loop(n, _):
-        events(left + (n * behind) // chunks, left + ((n + 1) * behind) // chunks, late)
-        feed(pl.ds(pl.multiple_of(n * span, span), span))
-        return 0
-
-    lax.fori_loop(0, chunks, feed_loop, 0)
-    if units % span:
-        feed(pl.ds(units // span * span, units % span))
-    heads_out.wait_send()
-    wide_n = math.gcd(features, 256)
-
-    def down(n, _):
-        cols = pl.ds(pl.multiple_of(n * wide_n, wide_n), wide_n)
-        term[:, cols] = jnp.dot(
-            hidden[...], down_all[:, cols], preferred_element_type=f32
+    lax.fori_loop(0, 2 * chunks, feed_loop, 0)
+
+    @pl.when(has_extra)
+    def _():
+        def body(n, _):
+            gate_e = ext_all[:, 0].reshape(n_sp * gate_rows, extra)
+            up_e = ext_all[:, 1].reshape(n_sp * gate_rows, extra)
+            feed_from(group_rows(n), gate_e, up_e, pl.ds(main, extra))
+            return 0
+
+        lax.fori_loop(0, 2, body, 0)
+
+        def lay(i, _):
+            oz = i // layer
+            fy = jnp.abs(lax.rem(i // wide_x, wide_y) - my_y)
+            fx = jnp.abs(lax.rem(i, wide_x) - my_x)
+            slot = (fy * 2 + fx) * wide_z + oz
+            down_all[main:, pl.ds(pl.multiple_of(slot * down_cols, down_cols), down_cols)] = ext_all[i, 2]
+            return 0
+
+        lax.fori_loop(0, n_sp, lay, 0)
+
+    wide_k = wide_z * down_cols
+    wide_n = math.gcd(wide_k, 256)
+    pieces = wide_k // wide_n
+
+    def down_with(depth, k):
+        def body(n, _):
+            rows = group_rows(n // pieces)
+            cols = pl.ds(pl.multiple_of(k * wide_k + lax.rem(n, pieces) * wide_n, wide_n), wide_n)
+            term[rows, cols] = jnp.dot(
+                hidden[rows, :depth], down_all[:depth, cols], preferred_element_type=f32
+            ).astype(bf16)
+            return 0
+
+        lax.fori_loop(0, 2 * pieces, body, 0)
+
+    sums, sums_far = [], []
+    at_core = core * 2 * share
+
+    def pair_sums(k):
+        cols = pl.ds(k * wide_k, wide_k)
+        away = pl.ds(pl.multiple_of((1 - core) * 2 * share, share), 2 * share)
+        sums.append(to_pair(4 + k, term.at[away, cols], inbox2.at[:, cols]))
+        sums[k].start()
+
+    def far_sums(k):
+        cols = pl.ds(k * wide_k, wide_k)
+        sums[k].wait_recv()
+        theirs_at = pl.multiple_of((1 - side) * share, share)
+        psum[:, cols] = (
+            term[pl.ds(pl.multiple_of(at_core + theirs_at, share), share), cols].astype(f32)
+            + inbox2[pl.ds(theirs_at, share), cols].astype(f32)
         ).astype(bf16)
-        return 0
-
-    lax.fori_loop(0, features // wide_n, down, 0)
-    sums_out = to_pair(2, term.at[theirs], inbox2)
-    sums_out.start()
-
-    def sent(i, _):
-        origin = (i // strides[0], lax.rem(i // strides[1], wide_y), lax.rem(i, wide_x))
-        for w, way in enumerate(ways):
-            run(wanted(ORDER_C, origin, way), lambda w=w: lat_copy(w, i, False).wait_send())
-            for p, (order, _, _) in enumerate(parts):
-                run(wanted(order, origin, way), lambda p=p, w=w: part_copy(p, w, i, False).wait_send())
-        pl.when(i != me)(lambda: pair_lat(i).wait_send())
-        return 0
-
-    lax.fori_loop(0, n_sp, sent, 0)
-    rows_out.wait_send()
-    sums_out.wait_recv()
-
-    def finish(n, _):
-        rows = pl.ds(pl.multiple_of(n * rows_at_once, rows_at_once), rows_at_once)
-        full = pl.ds(pl.multiple_of(core * share + n * rows_at_once, rows_at_once), rows_at_once)
-        summed = term[full, :].astype(f32) + inbox2[rows, :].astype(f32)
-        out[rows, :] = (kept[rows, :].astype(f32) + 0.5 * summed).astype(bf16)
-        return 0
-
-    lax.fori_loop(0, share // rows_at_once, finish, 0)
-    sums_out.wait_send()
+        sums_far.append(to_partner(8 + k, psum.at[:, cols], inbox3.at[:, cols]))
+        sums_far[k].start()
+
+    groups = ((0, 0), (0, 1), (1, 0), (1, 1))
+    for k, (fy, fx) in enumerate(groups):
+        if k:
+            down_group(fy, fx)
+        run(has_extra, lambda k=k: down_with(main + extra, k))
+        run(jnp.logical_not(has_extra), lambda k=k: down_with(main, k))
+        pair_sums(k)
+        far_sums(k)
+
+    def drain(ref, sem):
+        pltpu.make_async_copy(ref, ref, sem).wait()
+
+    for z in range(wide_z):
+        @pl.when(my_z == z)
+        def _(z=z):
+            up = 1 if z + 1 < wide_z else 0
+            drain(lat_all.at[pl.ds(0, (up + 3) * (z + 1) * half)], lat_send.at[0])
+            drain(lat_all.at[pl.ds(0, (layer * (z + 1) - 1) * half)], lat_send.at[1])
+            two = (1 if z + 2 < wide_z else 0) + (1 if z >= 2 else 0)
+            one = up + (1 if z >= 1 else 0)
+            on = (z if z + 2 < wide_z else 0) + (wide_z - 1 - z if z >= 2 else 0)
+            n = two + one + on + 3 * wide_z
+            drain(gate_all.at[pl.ds(0, n * gate_rows)], send.at[0])
+            drain(up_all.at[pl.ds(0, n * gate_rows)], send.at[1])
+            drain(down_all.at[pl.ds(0, main), pl.ds(0, n * down_cols)], send.at[2])
+            run(has_extra, lambda: drain(ext_all.at[pl.ds(0, two + on + 3 * wide_z)], send.at[3]))
+            run(jnp.logical_not(has_extra), lambda: drain(ext_all.at[pl.ds(0, one)], send.at[3]))
+
+    for copy in [rows_out, rows_far, rows_on] + sums:
+        copy.wait_send()
+
+    mine_at = pl.multiple_of(side * share, share)
+    for k, (fy, fx) in enumerate(groups):
+        sums_far[k].wait_recv()
+
+        def finish(t, _, k=k, fy=fy, fx=fx):
+            slot = pl.ds(pl.multiple_of((k * wide_z + t) * down_cols, down_cols), down_cols)
+            i = (t * wide_y + my_y + fy * (1 - 2 * my_y)) * wide_x + my_x + fx * (1 - 2 * my_x)
+            cols = pl.ds(pl.multiple_of(i * down_cols, down_cols), down_cols)
+            summed = (
+                term[pl.ds(pl.multiple_of(at_core + mine_at, share), share), slot].astype(f32)
+                + inbox2[pl.ds(mine_at, share), slot].astype(f32)
+                + inbox3[:, slot].astype(f32)
+            )
+            out[:, cols] = (kept[:, cols].astype(f32) + 0.5 * summed).astype(bf16)
+            return 0
+
+        lax.fori_loop(0, wide_z, finish, 0)
+    for copy in sums_far:
+        copy.wait_send()
 
 
 def fused_shards(
@@ -636,6 +798,8 @@
     wob = out_broad.reshape(-1, features)
     heads = ql.shape[0] + qb.shape[0]
     units = gate_weight.shape[1]
+    extra = gate_weight.shape[0]
+    main = (units - extra) // 2
     wide_b = value_up_broad.shape[2]
     vmem = pl.BlockSpec(memory_space=pltpu.VMEM)
     args = (
@@ -648,14 +812,19 @@
         functools.partial(layer_kernel, grid, (tokens, share, rope)),
         out_shape=jax.ShapeDtypeStruct((share, features), bf16),
         in_specs=[
-            pl.BlockSpec(memory_space=pl.ANY) if k in (0, 12, 13) else vmem for k in range(len(args))
+            pl.BlockSpec(memory_space=pl.ANY) if k in (0, 12, 13, 14, 15, 16) else vmem for k in range(len(args))
         ],
         out_specs=vmem,
         scratch_shapes=[
-            pltpu.VMEM((n_sp, tokens + rope, rank), bf16),
-            pltpu.VMEM((features, units), bf16),
-            pltpu.VMEM((features, units), bf16),
-            pltpu.VMEM((units, features), bf16),
+            pltpu.VMEM((n_sp * (tokens + rope), rank), bf16),
+            pltpu.VMEM((features, main), bf16),
+            pltpu.VMEM((features, main), bf16),
+            pltpu.VMEM((main + extra, features), bf16),
+            pltpu.VMEM((n_sp, 3, extra, extra), bf16),
+            pltpu.VMEM(gate_weight.shape, bf16),
+            pltpu.VMEM(up_weight.shape, bf16),
+            pltpu.VMEM(down_weight.shape, bf16),
+            pltpu.VMEM((3, extra, extra), bf16),
             pltpu.VMEM(ql.shape, bf16),
             pltpu.VMEM(qb.shape, bf16),
             pltpu.VMEM(ql.shape, bf16),
@@ -667,23 +836,25 @@
             pltpu.VMEM((ql.shape[0], value_up_lean.shape[2], tokens), f32),
             pltpu.VMEM((qb.shape[0], wide_b, tokens), f32),
             pltpu.VMEM((tokens, vul.shape[0] + vub.shape[0]), bf16),
-            pltpu.VMEM((tokens, features), bf16),
+            pltpu.VMEM((2 * tokens, features), bf16),
             pltpu.VMEM((share, features), bf16),
             pltpu.VMEM((share, features), bf16),
-            pltpu.VMEM((tokens, features), bf16),
-            pltpu.VMEM((tokens, units), bf16),
+            pltpu.VMEM((2 * tokens, features), bf16),
+            pltpu.VMEM((2 * tokens, main + extra), bf16),
+            pltpu.VMEM((2 * share, features), bf16),
+            pltpu.VMEM((share, features), bf16),
             pltpu.VMEM((share, features), bf16),
             pltpu.VMEM(wol.shape, bf16),
             pltpu.VMEM(wob.shape, bf16),
             pltpu.VMEM(residual_in.shape, bf16),
             dma((n_sp,)),
+            dma((2,)),
+            dma((n_sp,)),
             dma((4, n_sp)),
-            dma((2, n_sp)),
-            dma((6, n_sp)),
-            dma((6, 4, n_sp)),
+            dma((4,)),
             dma((10,)),
-            dma((3,)),
-            dma((3,)),
+            dma((12,)),
+            dma((12,)),
         ],
         compiler_params=pltpu.CompilerParams(
             collective_id=0, has_side_effects=True, vmem_limit_bytes=62 * 2**20
@@ -692,7 +863,7 @@
 
 
 def fits(grid, mesh, args):
-    if grid is None or mesh.shape["tp"] != 2 or grid[1] != 2 or grid[2] != 2 or grid[0] > 8:
+    if grid is None or mesh.shape["tp"] != 2 or grid[1] != 2 or grid[2] != 2 or grid[0] not in (2, 4, 6, 8):
         return False
     n_sp = mesh.shape["sp"]
     tokens = args[1].shape[0] // n_sp
@@ -702,11 +873,11 @@
     wide_l, wide_b = args[6].shape[2], args[7].shape[2]
     rope = args[4].shape[1]
     return (
-        tokens % 128 == 0 and tokens <= 256 and share % 16 == 0 and units >= 256
-        and units % 64 == 0 and heads_l % 2 == 0 and 2 * wide_l == wide_b and wide_b % 128 == 0
+        tokens % 128 == 0 and tokens <= 256 and share % 16 == 0 and units >= 384
+        and units % 256 == 128 and heads_l % 2 == 0 and 2 * wide_l == wide_b and wide_b % 128 == 0
         and args[3].shape[1] == tokens and rope % 32 == 0 and (tokens + rope) % 32 == 0
         and heads_b > 0 and args[8].shape[2] == wide_l and args[9].shape[2] == wide_b
-        and (args[14].shape[0] // n_sp) % 16 == 0 and (args[16].shape[1] // n_sp) % 128 == 0
+        and args[14].shape[0] // n_sp == 128 and args[16].shape[1] // n_sp == 128
     )
 
 

time: 170 us -> 157 us (0.924)
  the two profiles are of different devices: /device:TPU:27 before, /device:TPU:12 now
where the time goes in v1:
time: 157 us; the launch traced here: 156 us
  Pallas kernels  146 us (93%)
  local copies, waits for them, and re-layouts  5.5 us (4%)
  other arithmetic  4.35 us (3%)
    pallas_call x1, Pallas kernels, fused_shards(): pl.pallas_call(functools.partial(layer_kernel, grid, (tokens, share, rope...  146 us
    unnamed x3, local copies, waits for them, and re-layouts  5.5 us

profile of v1, /device:TPU:12, one launch (start us, length us, event | category | flops | bytes accessed | tf_op | source)
XLA Modules:
  0.0 156.3 jit_solution(7895267035994372051)
XLA Ops:
  0.0 1.0 fusion
  1.1 0.7 convert_element_type.24
  1.8 0.1 fusion.8
  1.9 0.8 multiply_sine_fusion
  2.7 1.0 fusion.2
  3.7 0.7 pad_maximum_fusion.lat
  4.4 1.8 %copy.18 = bf16[256,4,128]{0,2,1:T(8,128)(2,1)} copy(bf16[256,4,128]{2,1,0:T(4,128)(2,1)} %param.24) | data formatting | bytes 524288 | tf_op args[7]
  6.2 1.8 %copy.19 = bf16[256,4,128]{0,2,1:T(8,128)(2,1)} copy(bf16[256,4,128]{2,1,0:T(4,128)(2,1)} %param.26) | data formatting | bytes 524288 | tf_op args[9]
  8.0 146.4 %shard_map.163 = bf16[128,2048]{1,0:T(8,128)(2,1)} custom-call(bf16[128,2048]{1,0:T(8,128)(2,1)} %res_in.1, bf16[4,96,256]{2,1,0:T(8,128)(2,1)} %bitcast.25, bf16[4,160,256]{2,1,0:T(8,128)(2,1)} %bitcast.24, bf16[288,256]{1,0:T(8,128)(2,1)} %pad_maximum_fusion.lat, f32[16,256]{1,0:T(8,128)} %get-tuple-element.8.cosine, f32[16,256]{1,0:T(8,128)} %get-tuple-element.7.sine, ...), custom_call_target="tpu_custom_call" | custom-call | tf_op jit(solution)/shard_map/pallas_call | solution.py:811
  154.4 1.9 %copy.21 = bf16[128,2048]{1,0:T(8,128)(2,1)} copy(bf16[128,2048]{1,0:T(8,128)(2,1)} %shard_map.163) | data formatting | bytes 1048576
  (4 shorter events, 0.0 us)

commit v2 on v1

--- a/solution.py
+++ b/solution.py
@@ -220,11 +220,11 @@
     return wide_z, wide_y, wide_x
 
 
-def hop_table(grid, past):
+def hop_table(grid):
     wide_z = grid[0]
     entries = [
         (dz, fy, fx)
-        for dz in range(1 - wide_z, 1 if past else wide_z)
+        for dz in range(1 - wide_z, wide_z)
         for fy in range(2)
         for fx in range(2)
         if (dz, fy, fx) != (0, 0, 0)
@@ -234,8 +234,8 @@
 
 
 def layer_kernel(
-    grid, shapes, res_in, qlt, qbt, lat, cosine, sine, ag, mg, kul, kub, vul, vub, wol_in, wob_in, gw, uw, dw, out,
-    lat_all, gate_all, up_all, down_all, ext_all, own_g, own_u, own_d, own_e, ql, qb, ktl, ktb, valt_l, valt_b,
+    grid, shapes, res_in, qlt, qbt, lat_in, rope_in, lg, ag, mg, kul, kub_in, vul, vub_in, wol_in, wob_in, gw, uw, dw, out,
+    lat, kub, vub, cosine, sine, lat_all, gate_all, up_all, down_all, ext_all, own_g, own_u, own_d, own_e, ql, qb, keyn, scores, weigh, valt_l, valt_b,
     peak, total, acc_l, acc_b, att, term, inbox, kept, rows_all, hidden, inbox2, psum, inbox3, wol, wob, res,
     lat_recv, lat_send, lat_pair, recv, send, own_sem, pair_send, pair_recv,
 ):
@@ -268,8 +268,8 @@
 
     gate_rows, units = gw.shape
     down_cols = dw.shape[1]
-    main = gate_all.shape[1]
-    extra = units - 2 * main
+    extra = ext_all.shape[2]
+    main = (units - extra) // 2
     fetch = [
         pltpu.make_async_copy(src, dst, own_sem.at[k])
         for k, (src, dst) in enumerate((
@@ -280,14 +280,22 @@
             (wol_in, wol), (wob_in, wob), (res_in, res),
         ))
     ]
-    lat_rows = lat.shape[0]
-    own_lat = pltpu.make_async_copy(
-        lat, lat_all.at[pl.ds(pl.multiple_of(me * lat_rows, lat_rows), lat_rows)], own_sem.at[len(fetch)]
-    )
     for copy in fetch:
         copy.start()
-    own_lat.start()
-
+    half_rope = rope // 2
+    lane = lax.broadcasted_iota(jnp.int32, (half_rope, tokens), 1)
+    line = lax.broadcasted_iota(jnp.int32, (half_rope, tokens), 0)
+    freqs = jnp.zeros((half_rope, tokens), f32)
+    for k in range(half_rope):
+        freqs = jnp.where(line == k, THETA ** (-2.0 * k / rope), freqs)
+    angle = (me * tokens + lane).astype(f32) * freqs
+    cosine[...] = jnp.cos(angle)
+    sine[...] = jnp.sin(angle)
+    lat[:tokens, :] = normalize(lat_in[...].astype(f32), lg[...]).astype(bf16)
+    one, two = rope_in[:half_rope, :].astype(f32), rope_in[half_rope:, :].astype(f32)
+    lat[tokens:tokens + half_rope, :] = (one * cosine[...] - two * sine[...]).astype(bf16)
+    lat[tokens + half_rope:, :] = (one * sine[...] + two * cosine[...]).astype(bf16)
+    lat_rows = lat.shape[0]
     barrier = pltpu.get_barrier_semaphore()
     for where in (flip_x, flip_y):
         pl.semaphore_signal(barrier, inc=1, device_id={"sp": where})
@@ -316,16 +324,15 @@
             recv_sem=lat_pair.at[i], device_id={"tp": 1 - core},
         )
 
-    def lat_forward(i, fy, fx, mine):
-        column = jnp.logical_and(fy == 0, fx == 0)
-        up = z_way(1)
-        run(jnp.logical_and(column, up[1]), lambda: lat_copy(i, mine, up[2]).start())
-        to_x = jnp.logical_or(column, jnp.logical_and(core == 1, jnp.logical_and(fy == 1, fx == 0)))
-        to_y = jnp.logical_or(column, jnp.logical_and(core == 0, jnp.logical_and(fy == 0, fx == 1)))
-        run(to_x, lambda: lat_copy(i, mine, flip_x).start())
-        run(to_y, lambda: lat_copy(i, mine, flip_y).start())
-
-    lat_forward(me, my_y * 0, my_x * 0, True)
+    def lat_up(i, mine):
+        _, exists, where = z_way(1)
+        run(exists, lambda: lat_copy(i, mine, where).start())
+
+    turn = jnp.where(core == 0, flip_x, flip_y)
+    away = jnp.where(core == 0, flip_y, flip_x)
+    lat_copy(me, True, turn).start()
+    lat_copy(me, True, away).start()
+    lat_up(me, True)
 
     per = 4
 
@@ -351,25 +358,28 @@
         ox = my_x + fx * (1 - 2 * my_x)
         return ((my_z + dz) * wide_y + oy) * wide_x + ox
 
-    past = hop_table(grid, True)
-    past_words = words_of(past)
-
-    def lat_event(n, _):
-        dz, fy, fx = origin_of(n, past_words)
-
-        @pl.when(my_z + dz >= 0)
+    def lat_event(i, on):
+        lat_copy(i, False, turn).wait_recv()
+        if on:
+            lat_copy(i, False, away).start()
+        lat_up(i, False)
+        pair_lat(i).start()
+
+    def lat_layer(down):
+        @pl.when(my_z >= down)
         def _():
-            i = index_of(dz, fy, fx)
-            lat_copy(i, False, flip_x).wait_recv()
-            lat_forward(i, fy, fx, False)
-            pair_lat(i).start()
-
-        return 0
-
-    lax.fori_loop(0, len(past), lat_event, 0)
+            def body(t, _):
+                lat_event(index_of(-down, t // 2, lax.rem(t, 2)), False)
+                return 0
+
+            lax.fori_loop(0, layer, body, 0)
+
+    lat_event(turn, True)
+    lat_event(away, False)
+    lat_event(index_of(0, 1, 1), False)
 
     def slot_at(ref, i):
-        return ref.at[pl.ds(pl.multiple_of(i * gate_rows, gate_rows), gate_rows)]
+        return ref.at[pl.ds(pl.multiple_of(i * gate_rows, gate_rows), gate_rows), pl.ds(0, main)]
 
     def down_slot(dz, fy, fx):
         slot = (fy * 2 + fx) * wide_z + my_z + dz
@@ -401,7 +411,6 @@
         )
 
     has_extra = core == side
-    x_first = (True, False, core == 0, False)
 
     def to_z(p, src, step, origin, i, condition=True):
         _, exists, where = z_way(step)
@@ -416,24 +425,25 @@
             return down_slot(*seen(origin, fy, fx))
         return place(p, *origin)
 
-    def send_own(p):
+    def send_own(p, steps, in_layer, when=True):
         here = (0, 0, 0)
         mine = own_half(p, side)
         other = own_half(p, 1 - side)
         same = has_extra if p == 3 else True
         cross = jnp.logical_not(has_extra) if p == 3 else True
-        for step in (1, -1):
-            to_z(p, other, step, here, me, cross)
-        for step in (2, -2):
-            to_z(p, mine, step, here, me, same)
+        for step in steps:
+            if step in (1, -1):
+                to_z(p, other, step, here, me, jnp.logical_and(cross, when))
+            else:
+                to_z(p, mine, step, here, me, jnp.logical_and(same, when))
 
         def flips():
             part_copy(p, mine, dst_for(p, here, 0, 1), me, flip_x).start()
             part_copy(p, mine, dst_for(p, here, 1, 0), me, flip_y).start()
 
-        if p == 3:
+        if in_layer and p == 3:
             run(has_extra, flips)
-        else:
+        elif in_layer:
             flips()
 
     def part_event(p, dz, fy, fx):
@@ -446,127 +456,170 @@
         to_z(p, here, -2, origin, i, jnp.logical_and(column, dz > 0))
         x_line = jnp.logical_and(fy == 0, fx == 1)
         y_line = jnp.logical_and(fy == 1, fx == 0)
-        if x_first[p] is True:
+        if p == 0:
             to_x, to_y = column, jnp.logical_or(column, x_line)
-        elif x_first[p] is False:
+        elif p == 1:
             to_x, to_y = jnp.logical_or(column, y_line), column
         else:
-            to_x = jnp.logical_or(column, jnp.logical_and(y_line, jnp.logical_not(x_first[p])))
-            to_y = jnp.logical_or(column, jnp.logical_and(x_line, x_first[p]))
+            x_first = core == 0 if p == 2 else lax.rem(my_z + dz, 2) == 0
+            to_x = jnp.logical_or(column, jnp.logical_and(y_line, jnp.logical_not(x_first)))
+            to_y = jnp.logical_or(column, jnp.logical_and(x_line, x_first))
         run(to_x, lambda: part_copy(p, here, dst_for(p, origin, 0, 1), i, flip_x).start())
         run(to_y, lambda: part_copy(p, here, dst_for(p, origin, 1, 0), i, flip_y).start())
 
     for copy in fetch[:6]:
         copy.wait()
-    for p in (0, 1, 3):
-        send_own(p)
-
-    whole = hop_table(grid, False)
+    everything = (0, 1, 3, 2)
+    for p in everything:
+        send_own(p, (-1, -2), True)
+    lat_layer(1)
+    for p in everything:
+        send_own(p, (1, 2), False, my_z <= 1)
+
+    whole = hop_table(grid)
     whole_words = words_of(whole)
-
-    def gate_event(n, _):
-        dz, fy, fx = origin_of(n, whole_words)
-
-        @pl.when(jnp.logical_and(my_z + dz >= 0, my_z + dz < wide_z))
-        def _():
-            part_event(0, dz, fy, fx)
-            part_event(1, dz, fy, fx)
-            run(has_extra, lambda: part_event(3, dz, fy, fx))
-
-        return 0
-
-    def down_group(fy, fx):
+    count = len(whole)
+    hops = [abs(dz) + fy + fx for dz, fy, fx in whole]
+    early = sum(1 for hop in hops if hop <= 2)
+    lag = sum(1 for hop in hops if hop >= wide_z)
+
+    def events(low, high):
+        def gates(n):
+            dz, fy, fx = origin_of(n, whole_words)
+
+            @pl.when(jnp.logical_and(my_z + dz >= 0, my_z + dz < wide_z))
+            def _():
+                part_event(0, dz, fy, fx)
+                part_event(1, dz, fy, fx)
+                run(has_extra, lambda: part_event(3, dz, fy, fx))
+
+        def downs(n):
+            dz, fy, fx = origin_of(n, whole_words)
+            run(
+                jnp.logical_and(my_z + dz >= 0, my_z + dz < wide_z),
+                lambda: part_event(2, dz, fy, fx),
+            )
+
         def body(t, _):
-            dz = jnp.where(lax.rem(t, 2) == 1, -((t + 1) // 2), t // 2)
-            ok = jnp.logical_and(my_z + dz >= 0, my_z + dz < wide_z)
-            if (fy, fx) == (0, 0):
-                ok = jnp.logical_and(ok, dz != 0)
-            run(ok, lambda: part_event(2, dz, jnp.int32(fy), jnp.int32(fx)))
+            run(t < count, lambda: gates(t))
+            run(t >= lag, lambda: downs(t - lag))
             return 0
 
-        lax.fori_loop(0, 2 * wide_z - 1, body, 0)
+        lax.fori_loop(low, high, body, 0)
 
     own_rows = pl.ds(pl.multiple_of(me * gate_rows, gate_rows), gate_rows)
     own_lanes = pl.ds(pl.multiple_of(side * main, extra), main)
-    gate_all[own_rows, :] = own_g[:, own_lanes]
-    up_all[own_rows, :] = own_u[:, own_lanes]
+    gate_all[own_rows, :main] = own_g[:, own_lanes]
+    up_all[own_rows, :main] = own_u[:, own_lanes]
     down_all[:main, pl.ds(pl.multiple_of(my_z * down_cols, down_cols), down_cols)] = own_d[own_lanes, :]
     ext_all[me] = own_e[...]
 
-    half_rope = rope // 2
+    wide_l = kul.shape[0] // heads_l
+    wide_b = kub.shape[1] // heads_b
+    for h in range(heads_b):
+        part = slice(h * wide_b, (h + 1) * wide_b)
+        kub[:, part] = kub_in[:, h, :]
+        vub[part, :] = vub_in[:, h, :].T
     for given, query in ((qlt, ql), (qbt, qb)):
         nope = given.shape[1] - rope
         for h in range(given.shape[0]):
             one = given[h, nope:nope + half_rope, :].astype(f32)
             two = given[h, nope + half_rope:, :].astype(f32)
-            query[h, :nope, :] = given[h, :nope, :]
-            query[h, nope:nope + half_rope, :] = (one * cosine[...] - two * sine[...]).astype(bf16)
-            query[h, nope + half_rope:, :] = (one * sine[...] + two * cosine[...]).astype(bf16)
-    own_lat.wait()
-
-    def lat_arrived(i, _):
-        ours = jnp.logical_and(i != me, i < (my_z + 1) * layer)
-        run(ours, lambda: pair_lat(i).wait_recv())
-        return 0
-
-    lax.fori_loop(0, n_sp, lat_arrived, 0)
+            if nope < wide_b:
+                query[h, :wide_b, :] = jnp.zeros((wide_b, tokens), bf16)
+            at = (h * nope) % wide_b
+            query[h, at:at + nope, :] = given[h, :nope, :]
+            query[h, wide_b:wide_b + half_rope, :] = (one * cosine[...] - two * sine[...]).astype(bf16)
+            query[h, wide_b + half_rope:, :] = (one * sine[...] + two * cosine[...]).astype(bf16)
+    lat_all[pl.ds(pl.multiple_of(me * lat_rows, 16), lat_rows), :] = lat[...]
 
     peak[...] = jnp.full(peak.shape, NEGATIVE, f32)
     total[...] = jnp.zeros(total.shape, f32)
     acc_l[...] = jnp.zeros(acc_l.shape, f32)
     acc_b[...] = jnp.zeros(acc_b.shape, f32)
-    wide_l = kul.shape[0] // heads_l
-    wide_b = kub.shape[0] // heads_b
     contract = (((1,), (1,)), ((), ()))
-    contract_rows = (((0,), (0,)), ((), ()))
+    strip = math.gcd(tokens, 64)
+    strips = [slice(at, at + strip) for at in range(0, tokens, strip)]
 
     def attend_block(j, masked):
         at_j = pl.multiple_of(j * lat_rows, 16)
         rows = lat_all[pl.ds(at_j, tokens), :]
-        rot = lat_all[pl.ds(pl.multiple_of(at_j + tokens, 16), rope), :]
-        for ups, keys, heads, wide in ((kul, ktl, heads_l, wide_l), (kub, ktb, heads_b, wide_b)):
-            made = lax.dot_general(ups[...], rows, contract, preferred_element_type=f32).astype(bf16)
-            for h in range(heads):
-                keys[h, :wide, :] = made[h * wide:(h + 1) * wide]
-                keys[h, wide:, :] = rot
+        rot = lat_all[pl.ds(pl.multiple_of(at_j + tokens, 16), rope), :].T
+        split = heads_l * wide_l
+        keyn[:, :split] = lax.dot_general(rows, kul[...], contract, preferred_element_type=f32).astype(bf16)
+        keyn[:, split:] = jnp.dot(rows, kub[...], preferred_element_type=f32).astype(bf16)
         for ups, held in ((vul, valt_l), (vub, valt_b)):
             held[...] = lax.dot_general(
                 ups[...], rows, contract, preferred_element_type=f32
             ).astype(bf16)
-        if masked:
-            key_pos = lax.broadcasted_iota(jnp.int32, (tokens, tokens), 0)
-            visible = key_pos <= lax.broadcasted_iota(jnp.int32, (tokens, tokens), 1)
+
+        def of(g):
+            if g < heads_l:
+                return g, ql, valt_l, acc_l, wide_l, wide_l + rope
+            return g - heads_l, qb, valt_b, acc_b, wide_b, wide_b + rope
+
+        def score(g):
+            h, query = of(g)[:2]
+            at = (g * wide_l // wide_b if g < heads_l else split // wide_b + h) * wide_b
+            keys = jnp.concatenate([keyn[:, at:at + wide_b], rot], axis=1)
+            held = jnp.dot(keys, query[h], preferred_element_type=f32)
+            if masked:
+                key_pos = lax.broadcasted_iota(jnp.int32, (tokens, tokens), 0)
+                visible = key_pos <= lax.broadcasted_iota(jnp.int32, (tokens, tokens), 1)
+                held = jnp.where(visible, held, NEGATIVE)
+            scores[g % 2] = held
+
+        score(0)
         for g in range(heads_l + heads_b):
-            if g < heads_l:
-                h, query, keys, held, acc, wide = g, ql, ktl, valt_l, acc_l, wide_l
-            else:
-                h, query, keys, held, acc, wide = g - heads_l, qb, ktb, valt_b, acc_b, wide_b
-            scores = lax.dot_general(
-                keys[h], query[h], contract_rows, preferred_element_type=f32
-            ) * (LOG2E * query.shape[1] ** (-0.5))
-            if masked:
-                scores = jnp.where(visible, scores, NEGATIVE)
+            if g + 1 < heads_l + heads_b:
+                score(g + 1)
+            h, query, held, acc, wide, size = of(g)
+            scale = LOG2E * size ** (-0.5)
             old = peak[g]
-            new = jnp.maximum(old, jnp.max(scores, axis=0, keepdims=True))
-            weights = jnp.exp2(scores - new)
+            top = jnp.max(scores[g % 2, strips[0], :], axis=0, keepdims=True)
+            for part in strips[1:]:
+                top = jnp.maximum(top, jnp.max(scores[g % 2, part, :], axis=0, keepdims=True))
+            new = jnp.maximum(old, top * scale)
             factor = jnp.exp2(old - new)
+            summed = total[g] * factor
+            for part in strips:
+                weights = jnp.exp2(scores[g % 2, part, :] * scale - new)
+                summed = summed + jnp.sum(weights, axis=0, keepdims=True)
+                weigh[g % 2, part, :] = weights.astype(bf16)
             peak[g] = new
-            total[g] = total[g] * factor + jnp.sum(weights, axis=0, keepdims=True)
+            total[g] = summed
             acc[h] = acc[h] * factor + jnp.dot(
-                held[h * wide:(h + 1) * wide, :], weights.astype(bf16), preferred_element_type=f32
+                held[h * wide:(h + 1) * wide, :], weigh[g % 2], preferred_element_type=f32
             )
 
-    def step(j, _):
-        lax.fori_loop((j * early) // n_sp, ((j + 1) * early) // n_sp, gate_event, 0)
-        pl.when(j < me)(lambda: attend_block(j, False))
+    def attend_layer(down, low, high):
+        def body(t, _):
+            events(low + (t * (high - low)) // layer, low + ((t + 1) * (high - low)) // layer)
+            i = (my_z - down) * layer + t
+
+            @pl.when(jnp.logical_and(my_z >= down, i < me))
+            def _():
+                pair_lat(i).wait_recv()
+                attend_block(i, False)
+
+            return 0
+
+        lax.fori_loop(0, layer, body, 0)
+
+    attend_block(me, True)
+    attend_layer(0, 0, 0)
+    for down in range(1, wide_z):
+        if down + 1 < wide_z:
+            lat_layer(down + 1)
+            for p in everything:
+                send_own(p, (1, 2), False, my_z == down + 1)
+        attend_layer(down, (down - 1) * early // (wide_z - 1), down * early // (wide_z - 1))
+
+    def rest(i, _):
+        run(jnp.logical_and(i > me, i < (my_z + 1) * layer), lambda: pair_lat(i).wait_recv())
         return 0
 
-    count = len(whole)
-    early = sum(1 for dz, fy, fx in whole if abs(dz) + fy + fx <= 2)
-    lax.fori_loop(0, n_sp, step, 0)
-    attend_block(me, True)
-    send_own(2)
-    lax.fori_loop(early, count, gate_event, 0)
+    lax.fori_loop(0, n_sp, rest, 0)
 
     split = heads_l * wide_l
     for heads, wide, acc, base, col in (
@@ -634,6 +687,8 @@
     rows_out.start()
     rows_far.start()
     heads_out.wait_send()
+    ready = sum(1 for hop in hops if hop < wide_z)
+    events(early, ready)
     far_at = rows_all.at[place_of(core, 1 - side)]
     to_partner(2, far_at, far_at).wait_recv()
     rows_on = to_pair(3, far_at, far_at)
@@ -642,19 +697,34 @@
     to_pair(1, near_at, near_at).wait_recv()
     last_at = rows_all.at[place_of(1 - core, 1 - side)]
     to_pair(3, last_at, last_at).wait_recv()
-    down_group(0, 0)
+    events(ready, count)
 
     def feed_from(rows, gate_w, up_w, cols):
         gate = jnp.dot(rows_all[rows, :], gate_w, preferred_element_type=f32)
         up = jnp.dot(rows_all[rows, :], up_w, preferred_element_type=f32)
         hidden[rows, cols] = (gate / (1.0 + jnp.exp(-gate)) * up).astype(bf16)
 
-    span = math.gcd(main, 256)
+    span = 256
     chunks = main // span
-    group = 2 * tokens // 2
+    group = tokens
 
     def group_rows(n):
         return pl.ds(pl.multiple_of(n * group, group), group)
+
+    @pl.when(has_extra)
+    def _():
+        def lay(i, _):
+            oz = i // layer
+            fy = jnp.abs(lax.rem(i // wide_x, wide_y) - my_y)
+            fx = jnp.abs(lax.rem(i, wide_x) - my_x)
+            slot = (fy * 2 + fx) * wide_z + oz
+            at_i = pl.ds(pl.multiple_of(i * gate_rows, gate_rows), gate_rows)
+            gate_all[at_i, main:] = ext_all[i, 0]
+            up_all[at_i, main:] = ext_all[i, 1]
+            down_all[main:, pl.ds(pl.multiple_of(slot * down_cols, down_cols), down_cols)] = ext_all[i, 2]
+            return 0
+
+        lax.fori_loop(0, n_sp, lay, 0)
 
     def feed_loop(n, _):
         rows = group_rows(n // chunks)
@@ -664,25 +734,17 @@
 
     lax.fori_loop(0, 2 * chunks, feed_loop, 0)
 
-    @pl.when(has_extra)
-    def _():
+    def feed_rest(high):
         def body(n, _):
-            gate_e = ext_all[:, 0].reshape(n_sp * gate_rows, extra)
-            up_e = ext_all[:, 1].reshape(n_sp * gate_rows, extra)
-            feed_from(group_rows(n), gate_e, up_e, pl.ds(main, extra))
+            cols = slice(chunks * span, high)
+            feed_from(group_rows(n), gate_all[:, cols], up_all[:, cols], cols)
             return 0
 
-        lax.fori_loop(0, 2, body, 0)
-
-        def lay(i, _):
-            oz = i // layer
-            fy = jnp.abs(lax.rem(i // wide_x, wide_y) - my_y)
-            fx = jnp.abs(lax.rem(i, wide_x) - my_x)
-            slot = (fy * 2 + fx) * wide_z + oz
-            down_all[main:, pl.ds(pl.multiple_of(slot * down_cols, down_cols), down_cols)] = ext_all[i, 2]
-            return 0
-
-        lax.fori_loop(0, n_sp, lay, 0)
+        if high > chunks * span:
+            lax.fori_loop(0, 2, body, 0)
+
+    run(has_extra, lambda: feed_rest(main + extra))
+    run(jnp.logical_not(has_extra), lambda: feed_rest(main))
 
     wide_k = wide_z * down_cols
     wide_n = math.gcd(wide_k, 256)
@@ -720,13 +782,18 @@
         sums_far[k].start()
 
     groups = ((0, 0), (0, 1), (1, 0), (1, 1))
+    last = sum(1 for hop in hops if hop > wide_z)
     for k, (fy, fx) in enumerate(groups):
-        if k:
-            down_group(fy, fx)
+        if k == 1:
+            events(count, count + lag - last)
+        if k == 3:
+            events(count + lag - last, count + lag)
         run(has_extra, lambda k=k: down_with(main + extra, k))
         run(jnp.logical_not(has_extra), lambda k=k: down_with(main, k))
         pair_sums(k)
-        far_sums(k)
+        if k:
+            far_sums(k - 1)
+    far_sums(len(groups) - 1)
 
     def drain(ref, sem):
         pltpu.make_async_copy(ref, ref, sem).wait()
@@ -735,14 +802,14 @@
         @pl.when(my_z == z)
         def _(z=z):
             up = 1 if z + 1 < wide_z else 0
-            drain(lat_all.at[pl.ds(0, (up + 3) * (z + 1) * half)], lat_send.at[0])
+            drain(lat_all.at[pl.ds(0, (up * layer * (z + 1) + 3) * half)], lat_send.at[0])
             drain(lat_all.at[pl.ds(0, (layer * (z + 1) - 1) * half)], lat_send.at[1])
             two = (1 if z + 2 < wide_z else 0) + (1 if z >= 2 else 0)
             one = up + (1 if z >= 1 else 0)
             on = (z if z + 2 < wide_z else 0) + (wide_z - 1 - z if z >= 2 else 0)
             n = two + one + on + 3 * wide_z
-            drain(gate_all.at[pl.ds(0, n * gate_rows)], send.at[0])
-            drain(up_all.at[pl.ds(0, n * gate_rows)], send.at[1])
+            drain(gate_all.at[pl.ds(0, n * gate_rows), pl.ds(0, main)], send.at[0])
+            drain(up_all.at[pl.ds(0, n * gate_rows), pl.ds(0, main)], send.at[1])
             drain(down_all.at[pl.ds(0, main), pl.ds(0, n * down_cols)], send.at[2])
             run(has_extra, lambda: drain(ext_all.at[pl.ds(0, two + on + 3 * wide_z)], send.at[3]))
             run(jnp.logical_not(has_extra), lambda: drain(ext_all.at[pl.ds(0, one)], send.at[3]))
@@ -782,29 +849,21 @@
     rank = latent.shape[1]
     rope = rope_key.shape[1]
     n_sp = lax.axis_size("sp")
-    positions = lax.axis_index("sp") * tokens + jnp.arange(tokens, dtype=jnp.int32)
-
     ql, qb = (jnp.transpose(query, (1, 2, 0)) for query in (query_lean, query_broad))
-    freqs = THETA ** (-2.0 * jnp.arange(rope // 2, dtype=f32) / rope)
-    angle = freqs[:, None] * positions.astype(f32)[None, :]
-    lat = normalize(latent.astype(f32), latent_gain).astype(bf16)
-    rot_key = rotate(rope_key.astype(f32), positions).astype(bf16)
-    lat = jnp.concatenate([lat, rot_key.T], axis=0)
     kul = key_up_lean.reshape(rank, -1).T
-    kub = key_up_broad.reshape(rank, -1).T
     vul = value_up_lean.reshape(rank, -1).T
-    vub = value_up_broad.reshape(rank, -1).T
     wol = out_lean.reshape(-1, features)
     wob = out_broad.reshape(-1, features)
     heads = ql.shape[0] + qb.shape[0]
+    wide_all = qb.shape[0] * value_up_broad.shape[2]
     units = gate_weight.shape[1]
     extra = gate_weight.shape[0]
     main = (units - extra) // 2
     wide_b = value_up_broad.shape[2]
     vmem = pl.BlockSpec(memory_space=pltpu.VMEM)
     args = (
-        residual_in, ql, qb, lat, jnp.cos(angle), jnp.sin(angle), attn_gain[None], mlp_gain[None],
-        kul, kub, vul, vub, wol, wob,
+        residual_in, ql, qb, latent, rope_key.T, latent_gain[None], attn_gain[None], mlp_gain[None],
+        kul, key_up_broad, vul, value_up_broad, wol, wob,
         gate_weight, up_weight, down_weight,
     )
     dma = pltpu.SemaphoreType.DMA
@@ -816,26 +875,32 @@
         ],
         out_specs=vmem,
         scratch_shapes=[
+            pltpu.VMEM((tokens + rope, rank), bf16),
+            pltpu.VMEM((rank, wide_all), bf16),
+            pltpu.VMEM((wide_all, rank), bf16),
+            pltpu.VMEM((rope // 2, tokens), f32),
+            pltpu.VMEM((rope // 2, tokens), f32),
             pltpu.VMEM((n_sp * (tokens + rope), rank), bf16),
-            pltpu.VMEM((features, main), bf16),
-            pltpu.VMEM((features, main), bf16),
+            pltpu.VMEM((features, main + extra), bf16),
+            pltpu.VMEM((features, main + extra), bf16),
             pltpu.VMEM((main + extra, features), bf16),
             pltpu.VMEM((n_sp, 3, extra, extra), bf16),
             pltpu.VMEM(gate_weight.shape, bf16),
             pltpu.VMEM(up_weight.shape, bf16),
             pltpu.VMEM(down_weight.shape, bf16),
             pltpu.VMEM((3, extra, extra), bf16),
-            pltpu.VMEM(ql.shape, bf16),
+            pltpu.VMEM((ql.shape[0],) + qb.shape[1:], bf16),
             pltpu.VMEM(qb.shape, bf16),
-            pltpu.VMEM(ql.shape, bf16),
-            pltpu.VMEM(qb.shape, bf16),
+            pltpu.VMEM((tokens, kul.shape[0] + wide_all), bf16),
+            pltpu.VMEM((2, tokens, tokens), f32),
+            pltpu.VMEM((2, tokens, tokens), bf16),
             pltpu.VMEM((vul.shape[0], tokens), bf16),
-            pltpu.VMEM((vub.shape[0], tokens), bf16),
+            pltpu.VMEM((wide_all, tokens), bf16),
             pltpu.VMEM((heads, 1, tokens), f32),
             pltpu.VMEM((heads, 1, tokens), f32),
             pltpu.VMEM((ql.shape[0], value_up_lean.shape[2], tokens), f32),
             pltpu.VMEM((qb.shape[0], wide_b, tokens), f32),
-            pltpu.VMEM((tokens, vul.shape[0] + vub.shape[0]), bf16),
+            pltpu.VMEM((tokens, vul.shape[0] + wide_all), bf16),
             pltpu.VMEM((2 * tokens, features), bf16),
             pltpu.VMEM((share, features), bf16),
             pltpu.VMEM((share, features), bf16),

time: 157 us -> 118 us (0.75)
  the two profiles are of different devices: /device:TPU:12 before, /device:TPU:17 now
where the time goes in v2:
time: 118 us; the launch traced here: 116 us
  Pallas kernels  114 us (97%)
  local copies, waits for them, and re-layouts  1.88 us (2%)
    pallas_call x1, Pallas kernels, fused_shards(): pl.pallas_call(functools.partial(layer_kernel, grid, (tokens, share, rope...  114 us

profile of v2, /device:TPU:17, one launch (start us, length us, event | category | flops | bytes accessed | tf_op | source)
XLA Modules:
  0.0 116.1 jit_solution(1630758396142888769)
XLA Ops:
  0.0 114.2 %shard_map.163 = bf16[128,2048]{1,0:T(8,128)(2,1)} custom-call(bf16[128,2048]{1,0:T(8,128)(2,1)} %res_in.1, bf16[4,96,256]{2,1,0:T(8,128)(2,1)} %bitcast.17, bf16[4,160,256]{2,1,0:T(8,128)(2,1)} %bitcast.16, bf16[256,256]{1,0:T(8,128)(2,1)} %lat_in.1, bf16[32,256]{1,0:T(8,128)(2,1)} %bitcast.20, f32[1,256]{1,0:T(1,128)} %bitcast.23, f32[1,2048]{1,0:T(1,128)} %bitcast.21, ...), custom_call_target="tpu_custom_call" | custom-call | tf_op jit(solution)/shard_map/pallas_call | solution.py:870
  114.2 1.9 %copy.19 = bf16[128,2048]{1,0:T(8,128)(2,1)} copy(bf16[128,2048]{1,0:T(8,128)(2,1)} %shard_map.163) | data formatting | bytes 1048576

commit v3 on v2

--- a/solution.py
+++ b/solution.py
@@ -257,7 +257,7 @@
     z_ways = [
         (step, my_z + step < wide_z if step > 0 else my_z + step >= 0,
          jnp.clip(me + step * layer, 0, n_sp - 1))
-        for step in (1, -1, 2, -2)
+        for step in (1, -1, 2, -2, 3, -3)
     ]
 
     def z_way(step):
@@ -324,15 +324,16 @@
             recv_sem=lat_pair.at[i], device_id={"tp": 1 - core},
         )
 
-    def lat_up(i, mine):
+    turn = jnp.where(core == 0, flip_x, flip_y)
+    away = jnp.where(core == 0, flip_y, flip_x)
+
+    def lat_spread(i, mine):
         _, exists, where = z_way(1)
         run(exists, lambda: lat_copy(i, mine, where).start())
-
-    turn = jnp.where(core == 0, flip_x, flip_y)
-    away = jnp.where(core == 0, flip_y, flip_x)
-    lat_copy(me, True, turn).start()
-    lat_copy(me, True, away).start()
-    lat_up(me, True)
+        lat_copy(i, mine, turn).start()
+        lat_copy(i, mine, away).start()
+
+    lat_spread(me, True)
 
     per = 4
 
@@ -358,25 +359,28 @@
         ox = my_x + fx * (1 - 2 * my_x)
         return ((my_z + dz) * wide_y + oy) * wide_x + ox
 
-    def lat_event(i, on):
+    def lat_event(dz, fy, fx, column, line):
+        i = index_of(dz, fy, fx)
         lat_copy(i, False, turn).wait_recv()
-        if on:
+        if column:
+            lat_spread(i, False)
+        if line:
             lat_copy(i, False, away).start()
-        lat_up(i, False)
         pair_lat(i).start()
 
-    def lat_layer(down):
-        @pl.when(my_z >= down)
-        def _():
-            def body(t, _):
-                lat_event(index_of(-down, t // 2, lax.rem(t, 2)), False)
-                return 0
-
-            lax.fori_loop(0, layer, body, 0)
-
-    lat_event(turn, True)
-    lat_event(away, False)
-    lat_event(index_of(0, 1, 1), False)
+    def lat_column(down):
+        run(my_z >= down, lambda: lat_event(-down, 0, 0, True, False))
+
+    def lat_side(down):
+        def events_of():
+            near = jnp.where(core == 0, 0, 1)
+            lat_event(-down, near, 1 - near, False, True)
+            lat_event(-down, 1 - near, near, False, False)
+
+        run(my_z >= down, events_of)
+
+    def lat_far(down):
+        run(my_z >= down, lambda: lat_event(-down, 1, 1, False, False))
 
     def slot_at(ref, i):
         return ref.at[pl.ds(pl.multiple_of(i * gate_rows, gate_rows), gate_rows), pl.ds(0, main)]
@@ -432,7 +436,7 @@
         same = has_extra if p == 3 else True
         cross = jnp.logical_not(has_extra) if p == 3 else True
         for step in steps:
-            if step in (1, -1):
+            if step % 2:
                 to_z(p, other, step, here, me, jnp.logical_and(cross, when))
             else:
                 to_z(p, mine, step, here, me, jnp.logical_and(same, when))
@@ -452,8 +456,6 @@
         here = place(p, *origin)
         part_copy(p, here, here, i, flip_x).wait_recv()
         column = jnp.logical_and(fy == 0, fx == 0)
-        to_z(p, here, 2, origin, i, jnp.logical_and(column, dz < 0))
-        to_z(p, here, -2, origin, i, jnp.logical_and(column, dz > 0))
         x_line = jnp.logical_and(fy == 0, fx == 1)
         y_line = jnp.logical_and(fy == 1, fx == 0)
         if p == 0:
@@ -469,39 +471,55 @@
 
     for copy in fetch[:6]:
         copy.wait()
-    everything = (0, 1, 3, 2)
-    for p in everything:
-        send_own(p, (-1, -2), True)
-    lat_layer(1)
-    for p in everything:
-        send_own(p, (1, 2), False, my_z <= 1)
+    gates = (0, 1, 3, 2)
+    for p in gates:
+        send_own(p, (-1, -2, -3), False)
+        send_own(p, (1, 2, 3), False, my_z == 0)
+    lat_column(1)
+    for p in gates:
+        send_own(p, (1, 2, 3), False, my_z == 1)
+    lat_side(0)
+    if wide_z > 2:
+        lat_column(2)
+        for p in gates:
+            send_own(p, (1, 2, 3), False, my_z == 2)
+    lat_side(1)
+    for p in gates:
+        send_own(p, (), True)
+    lat_far(0)
+    lat_far(1)
 
     whole = hop_table(grid)
     whole_words = words_of(whole)
     count = len(whole)
     hops = [abs(dz) + fy + fx for dz, fy, fx in whole]
     early = sum(1 for hop in hops if hop <= 2)
-    lag = sum(1 for hop in hops if hop >= wide_z)
+    ready = sum(1 for hop in hops if hop < wide_z)
+    early = sum(1 for hop in hops if hop <= 2)
+    groups = ((0, 0), (0, 1), (1, 0), (1, 1))
+    grouped = whole
+    grouped_words = words_of(grouped)
+    lag = count - ready
+
+    def inside(dz):
+        return jnp.logical_and(my_z + dz >= 0, my_z + dz < wide_z)
 
     def events(low, high):
-        def gates(n):
+        def gate_parts(n):
             dz, fy, fx = origin_of(n, whole_words)
 
-            @pl.when(jnp.logical_and(my_z + dz >= 0, my_z + dz < wide_z))
+            @pl.when(inside(dz))
             def _():
                 part_event(0, dz, fy, fx)
                 part_event(1, dz, fy, fx)
                 run(has_extra, lambda: part_event(3, dz, fy, fx))
 
         def downs(n):
-            dz, fy, fx = origin_of(n, whole_words)
-            run(
-                jnp.logical_and(my_z + dz >= 0, my_z + dz < wide_z),
-                lambda: part_event(2, dz, fy, fx),
-            )
+            dz, fy, fx = origin_of(n, grouped_words)
+            run(inside(dz), lambda: part_event(2, dz, fy, fx))
 
         def body(t, _):
-            run(t < count, lambda: gates(t))
+            run(t < count, lambda: gate_parts(t))
             run(t >= lag, lambda: downs(t - lag))
             return 0
 
@@ -609,10 +627,13 @@
     attend_block(me, True)
     attend_layer(0, 0, 0)
     for down in range(1, wide_z):
-        if down + 1 < wide_z:
-            lat_layer(down + 1)
-            for p in everything:
-                send_own(p, (1, 2), False, my_z == down + 1)
+        if down == 1 and wide_z > 2:
+            lat_column(3)
+            lat_side(2)
+            lat_far(2)
+        if down == 2:
+            lat_side(3)
+            lat_far(3)
         attend_layer(down, (down - 1) * early // (wide_z - 1), down * early // (wide_z - 1))
 
     def rest(i, _):
@@ -662,7 +683,7 @@
         )
 
     def place_of(of_core, of_side):
-        return pl.ds(pl.multiple_of((of_core * 2 + of_side) * share, share), share)
+        return pl.ds(pl.multiple_of((of_side * 2 + of_core) * share, share), share)
 
     heads_out = to_pair(0, term.at[theirs], inbox)
     heads_out.start()
@@ -672,7 +693,7 @@
     def norms(n, _):
         rows = pl.ds(pl.multiple_of(n * rows_at_once, rows_at_once), rows_at_once)
         full = pl.ds(pl.multiple_of(core * share + n * rows_at_once, rows_at_once), rows_at_once)
-        spot = pl.ds(pl.multiple_of((core * 2 + side) * share + n * rows_at_once, rows_at_once), rows_at_once)
+        spot = pl.ds(pl.multiple_of((side * 2 + core) * share + n * rows_at_once, rows_at_once), rows_at_once)
         summed = term[full, :].astype(f32) + inbox[rows, :].astype(f32)
         branch = normalize(summed, ag[...])
         mixed = (res[rows, :].astype(f32) + branch).astype(bf16)
@@ -709,7 +730,8 @@
     group = tokens
 
     def group_rows(n):
-        return pl.ds(pl.multiple_of(n * group, group), group)
+        of_side = jnp.where(n == 0, 1 - side, side)
+        return pl.ds(pl.multiple_of(of_side * group, group), group)
 
     @pl.when(has_extra)
     def _():
@@ -726,74 +748,76 @@
 
         lax.fori_loop(0, n_sp, lay, 0)
 
-    def feed_loop(n, _):
-        rows = group_rows(n // chunks)
-        cols = pl.ds(pl.multiple_of(lax.rem(n, chunks) * span, span), span)
-        feed_from(rows, gate_all[:, cols], up_all[:, cols], cols)
-        return 0
-
-    lax.fori_loop(0, 2 * chunks, feed_loop, 0)
-
-    def feed_rest(high):
+    def feed(half):
+        rows = group_rows(half)
+
         def body(n, _):
+            cols = pl.ds(pl.multiple_of(n * span, span), span)
+            feed_from(rows, gate_all[:, cols], up_all[:, cols], cols)
+            return 0
+
+        lax.fori_loop(0, chunks, body, 0)
+
+        def rest(high):
             cols = slice(chunks * span, high)
-            feed_from(group_rows(n), gate_all[:, cols], up_all[:, cols], cols)
-            return 0
-
-        if high > chunks * span:
-            lax.fori_loop(0, 2, body, 0)
-
-    run(has_extra, lambda: feed_rest(main + extra))
-    run(jnp.logical_not(has_extra), lambda: feed_rest(main))
+            if high > chunks * span:
+                feed_from(rows, gate_all[:, cols], up_all[:, cols], cols)
+
+        run(has_extra, lambda: rest(main + extra))
+        run(jnp.logical_not(has_extra), lambda: rest(main))
 
     wide_k = wide_z * down_cols
     wide_n = math.gcd(wide_k, 256)
     pieces = wide_k // wide_n
 
-    def down_with(depth, k):
+    def down_with(depth, half, low, high):
+        rows = group_rows(half)
+
         def body(n, _):
-            rows = group_rows(n // pieces)
-            cols = pl.ds(pl.multiple_of(k * wide_k + lax.rem(n, pieces) * wide_n, wide_n), wide_n)
+            cols = pl.ds(pl.multiple_of(n * wide_n, wide_n), wide_n)
             term[rows, cols] = jnp.dot(
                 hidden[rows, :depth], down_all[:depth, cols], preferred_element_type=f32
             ).astype(bf16)
             return 0
 
-        lax.fori_loop(0, 2 * pieces, body, 0)
+        lax.fori_loop(low * pieces, high * pieces, body, 0)
+
+    def down(half, low, high):
+        run(has_extra, lambda: down_with(main + extra, half, low, high))
+        run(jnp.logical_not(has_extra), lambda: down_with(main, half, low, high))
 
     sums, sums_far = [], []
-    at_core = core * 2 * share
 
     def pair_sums(k):
         cols = pl.ds(k * wide_k, wide_k)
-        away = pl.ds(pl.multiple_of((1 - core) * 2 * share, share), 2 * share)
-        sums.append(to_pair(4 + k, term.at[away, cols], inbox2.at[:, cols]))
+        sums.append(to_pair(4 + k, term.at[place_of(1 - core, 1 - side), cols], inbox2.at[pl.ds(0, share), cols]))
         sums[k].start()
 
     def far_sums(k):
         cols = pl.ds(k * wide_k, wide_k)
         sums[k].wait_recv()
-        theirs_at = pl.multiple_of((1 - side) * share, share)
         psum[:, cols] = (
-            term[pl.ds(pl.multiple_of(at_core + theirs_at, share), share), cols].astype(f32)
-            + inbox2[pl.ds(theirs_at, share), cols].astype(f32)
+            term[place_of(core, 1 - side), cols].astype(f32) + inbox2[:share, cols].astype(f32)
         ).astype(bf16)
         sums_far.append(to_partner(8 + k, psum.at[:, cols], inbox3.at[:, cols]))
         sums_far[k].start()
 
-    groups = ((0, 0), (0, 1), (1, 0), (1, 1))
-    last = sum(1 for hop in hops if hop > wide_z)
+    feed(0)
+    since = count
     for k, (fy, fx) in enumerate(groups):
-        if k == 1:
-            events(count, count + lag - last)
-        if k == 3:
-            events(count + lag - last, count + lag)
-        run(has_extra, lambda k=k: down_with(main + extra, k))
-        run(jnp.logical_not(has_extra), lambda k=k: down_with(main, k))
+        until = lag + max(n + 1 for n, e in enumerate(grouped) if e[1:] == (fy, fx))
+        until = max(until, since)
+        events(max(since, count), max(until, count))
+        since = until
+        down(0, k, k + 1)
         pair_sums(k)
         if k:
             far_sums(k - 1)
     far_sums(len(groups) - 1)
+    feed(1)
+    down(1, 0, len(groups))
+    own_sums = to_pair(12, term.at[place_of(1 - core, side)], inbox2.at[pl.ds(share, share)])
+    own_sums.start()
 
     def drain(ref, sem):
         pltpu.make_async_copy(ref, ref, sem).wait()
@@ -802,22 +826,21 @@
         @pl.when(my_z == z)
         def _(z=z):
             up = 1 if z + 1 < wide_z else 0
-            drain(lat_all.at[pl.ds(0, (up * layer * (z + 1) + 3) * half)], lat_send.at[0])
+            drain(lat_all.at[pl.ds(0, (up + 3) * (z + 1) * half)], lat_send.at[0])
             drain(lat_all.at[pl.ds(0, (layer * (z + 1) - 1) * half)], lat_send.at[1])
             two = (1 if z + 2 < wide_z else 0) + (1 if z >= 2 else 0)
-            one = up + (1 if z >= 1 else 0)
-            on = (z if z + 2 < wide_z else 0) + (wide_z - 1 - z if z >= 2 else 0)
-            n = two + one + on + 3 * wide_z
+            odd = sum(1 for step in (1, -1, 3, -3) if 0 <= z + step < wide_z)
+            n = two + odd + 3 * wide_z
             drain(gate_all.at[pl.ds(0, n * gate_rows), pl.ds(0, main)], send.at[0])
             drain(up_all.at[pl.ds(0, n * gate_rows), pl.ds(0, main)], send.at[1])
             drain(down_all.at[pl.ds(0, main), pl.ds(0, n * down_cols)], send.at[2])
-            run(has_extra, lambda: drain(ext_all.at[pl.ds(0, two + on + 3 * wide_z)], send.at[3]))
-            run(jnp.logical_not(has_extra), lambda: drain(ext_all.at[pl.ds(0, one)], send.at[3]))
-
-    for copy in [rows_out, rows_far, rows_on] + sums:
+            run(has_extra, lambda: drain(ext_all.at[pl.ds(0, two + 3 * wide_z)], send.at[3]))
+            run(jnp.logical_not(has_extra), lambda: drain(ext_all.at[pl.ds(0, odd)], send.at[3]))
+
+    own_sums.wait_recv()
+    for copy in [rows_out, rows_far, rows_on, own_sums] + sums:
         copy.wait_send()
 
-    mine_at = pl.multiple_of(side * share, share)
     for k, (fy, fx) in enumerate(groups):
         sums_far[k].wait_recv()
 
@@ -826,8 +849,8 @@
             i = (t * wide_y + my_y + fy * (1 - 2 * my_y)) * wide_x + my_x + fx * (1 - 2 * my_x)
             cols = pl.ds(pl.multiple_of(i * down_cols, down_cols), down_cols)
             summed = (
-                term[pl.ds(pl.multiple_of(at_core + mine_at, share), share), slot].astype(f32)
-                + inbox2[pl.ds(mine_at, share), slot].astype(f32)
+                term[place_of(core, side), slot].astype(f32)
+                + inbox2[share:, slot].astype(f32)
                 + inbox3[:, slot].astype(f32)
             )
             out[:, cols] = (kept[:, cols].astype(f32) + 0.5 * summed).astype(bf16)
@@ -918,8 +941,8 @@
             dma((4, n_sp)),
             dma((4,)),
             dma((10,)),
-            dma((12,)),
-            dma((12,)),
+            dma((13,)),
+            dma((13,)),
         ],
         compiler_params=pltpu.CompilerParams(
             collective_id=0, has_side_effects=True, vmem_limit_bytes=62 * 2**20

time: 118 us -> 115 us (0.975); the launches traced: 116 us -> 115 us
    pallas_call x1, Pallas kernels: 114 us -> 113 us  [fused_shards(): pl.pallas_call(functools.partial(layer_kernel, grid, (tokens, share, rope...]
where the time goes in v3:
time: 115 us
  Pallas kernels  113 us (98%)
  local copies, waits for them, and re-layouts  1.88 us (2%)
    pallas_call x1, Pallas kernels, fused_shards(): pl.pallas_call(functools.partial(layer_kernel, grid, (tokens, share, rope...  113 us

profile of v3, /device:TPU:17, one launch (start us, length us, event | category | flops | bytes accessed | tf_op | source)
XLA Modules:
  0.0 114.5 jit_solution(17227128576678152857)
XLA Ops:
  0.0 112.6 %shard_map.163 = bf16[128,2048]{1,0:T(8,128)(2,1)} custom-call(bf16[128,2048]{1,0:T(8,128)(2,1)} %res_in.1, bf16[4,96,256]{2,1,0:T(8,128)(2,1)} %bitcast.17, bf16[4,160,256]{2,1,0:T(8,128)(2,1)} %bitcast.16, bf16[256,256]{1,0:T(8,128)(2,1)} %lat_in.1, bf16[32,256]{1,0:T(8,128)(2,1)} %bitcast.20, f32[1,256]{1,0:T(1,128)} %bitcast.23, f32[1,2048]{1,0:T(1,128)} %bitcast.21, ...), custom_call_target="tpu_custom_call" | custom-call | tf_op jit(solution)/shard_map/pallas_call | solution.py:893
  112.6 1.9 %copy.19 = bf16[128,2048]{1,0:T(8,128)(2,1)} copy(bf16[128,2048]{1,0:T(8,128)(2,1)} %shard_map.163) | data formatting | bytes 1048576

commit v4 on v3

--- a/solution.py
+++ b/solution.py
@@ -445,10 +445,8 @@
             part_copy(p, mine, dst_for(p, here, 0, 1), me, flip_x).start()
             part_copy(p, mine, dst_for(p, here, 1, 0), me, flip_y).start()
 
-        if in_layer and p == 3:
-            run(has_extra, flips)
-        elif in_layer:
-            flips()
+        if in_layer:
+            run(jnp.logical_and(same, when), flips)
 
     def part_event(p, dz, fy, fx):
         origin = (dz, fy, fx)
@@ -479,12 +477,16 @@
     for p in gates:
         send_own(p, (1, 2, 3), False, my_z == 1)
     lat_side(0)
+    for p in gates[:2]:
+        send_own(p, (), True, my_z == 2)
     if wide_z > 2:
         lat_column(2)
         for p in gates:
             send_own(p, (1, 2, 3), False, my_z == 2)
     lat_side(1)
-    for p in gates:
+    for p in gates[:2]:
+        send_own(p, (), True, my_z != 2)
+    for p in gates[2:]:
         send_own(p, (), True)
     lat_far(0)
     lat_far(1)

time: 115 us -> 114 us (level)
  no operation moved by 1% of the time
where the time goes in v4:
time: 114 us
  Pallas kernels  112 us (98%)
  local copies, waits for them, and re-layouts  1.88 us (2%)
    pallas_call x1, Pallas kernels, fused_shards(): pl.pallas_call(functools.partial(layer_kernel, grid, (tokens, share, rope...  112 us

profile of v4, /device:TPU:17, one launch (start us, length us, event | category | flops | bytes accessed | tf_op | source)
XLA Modules:
  0.0 114.3 jit_solution(11917194539156954186)
XLA Ops:
  0.0 112.4 %shard_map.163 = bf16[128,2048]{1,0:T(8,128)(2,1)} custom-call(bf16[128,2048]{1,0:T(8,128)(2,1)} %res_in.1, bf16[4,96,256]{2,1,0:T(8,128)(2,1)} %bitcast.17, bf16[4,160,256]{2,1,0:T(8,128)(2,1)} %bitcast.16, bf16[256,256]{1,0:T(8,128)(2,1)} %lat_in.1, bf16[32,256]{1,0:T(8,128)(2,1)} %bitcast.20, f32[1,256]{1,0:T(1,128)} %bitcast.23, f32[1,2048]{1,0:T(1,128)} %bitcast.21, ...), custom_call_target="tpu_custom_call" | custom-call | tf_op jit(solution)/shard_map/pallas_call | solution.py:895
  112.4 1.9 %copy.19 = bf16[128,2048]{1,0:T(8,128)(2,1)} copy(bf16[128,2048]{1,0:T(8,128)(2,1)} %shard_map.163) | data formatting | bytes 1048576
